TPU v7x, 128 devices: a whole 4x4x4 slice. The times are simulated.
128 devices in a mesh: sp: 16 (over z, y), tp: 8 (over x, core).
Axes of the slice: x: 4, y: 4, z: 4, core: 2. Of those that a mesh axis runs over, the one named last changes fastest.
Arguments:
- hidden: bfloat16 [16, 1024, 1024], P(None, 'sp'), may hold values from -0.09375 to 0.09375
- value_weight: bfloat16 [1024, 1024], P(None, 'tp'), may hold values from -0.75 to 0.75
- queries: bfloat16 [16, 8, 1024, 64], P(None, 'tp', 'sp'), may hold values from -0.1875 to 0.1875
- key_vectors: bfloat16 [16, 8, 1024, 64], P(None, 'tp', 'sp'), may hold values from -0.1875 to 0.1875
- forward_decay: float32 [16, 8, 1024, 64], P(None, 'tp', 'sp'), may hold values from -0.0029296875 to -9.765625e-06
- backward_decay: float32 [16, 8, 1024, 64], P(None, 'tp', 'sp'), may hold values from -0.0029296875 to -9.765625e-06
- cotangent: bfloat16 [16, 1024, 1024], P(None, 'sp', 'tp'), may hold values from -6 to 6
Outputs:
- grad_queries: bfloat16 [16, 8, 1024, 64], P(None, 'tp', 'sp')
- grad_keys: bfloat16 [16, 8, 1024, 64], P(None, 'tp', 'sp')
- grad_forward: float32 [16, 8, 1024, 64], P(None, 'tp', 'sp')
- grad_backward: float32 [16, 8, 1024, 64], P(None, 'tp', 'sp')
- grad_hidden: bfloat16 [16, 1024, 1024], P(None, 'sp', 'tp')
- grad_weight: float32 [1024, 1024], P('sp', 'tp')
All inputs are finite; a program needn't handle non-finite values.
Results may differ from a plain program's by a relative error of at most 0.015.
Values may be sent and summed in bfloat16 or wider, within the bound.
A program may use at most 128 MiB of HBM per device.

v0:
```python
import functools

import jax
import jax.numpy as jnp
from jax import lax
from jax.experimental import pallas as pl
from jax.experimental.pallas import tpu as pltpu
from jax.sharding import PartitionSpec as P

F32, BF16 = jnp.float32, jnp.bfloat16
MESH = pl.DeviceIdType.MESH
LAG = 2
EXTRA = 4


def dot(a, b, ca=1, cb=0):
    return lax.dot_general(a, b, (((ca,), (cb,)), ((), ())), preferred_element_type=F32)


def split(x):
    high = x.astype(BF16)
    return high, (x - high.astype(F32)).astype(BF16)


def plan(sp, batch, heads):
    outer = 4 if sp % 4 == 0 and batch % (sp // 4) == 0 else sp
    inner = sp // outer
    own = batch // inner
    return outer, inner, own, own * heads


def kernel(dims, hid, wgt, qry, key, fdec, bdec, cot,
           o_qk, o_fb, o_h, o_w,
           val, cum, intra_q, intra_k, intra_v,
           a_out, a_in, b_out, b_in, c_out, c_in, d_all, w_in, g_out, g_in,
           a_ss, a_rs, b_ss, b_rs, c_ss, c_rs, d_ss, d_rs, w_ss, w_rs, g_ss, g_rs):
    sp, tp, batch, heads, length, dk, dv, width = dims
    outer, inner, own, units = plan(sp, batch, heads)
    pack = 2 * dk
    feat = width // tp
    rows_sp = width // sp
    group = d_group(own)
    spi, tpi = lax.axis_index("sp"), lax.axis_index("tp")
    z, y = spi // inner, lax.rem(spi, inner)

    barrier = pltpu.get_barrier_semaphore()
    for r in range(1, sp):
        pl.semaphore_signal(barrier, inc=1, device_id={"sp": lax.rem(spi + r, sp)}, device_id_type=MESH)
    for r in range(1, tp):
        pl.semaphore_signal(barrier, inc=1, device_id={"tp": lax.rem(tpi + r, tp)}, device_id_type=MESH)
    pl.semaphore_wait(barrier, sp + tp - 2)

    def remote(src, dst, ss, rs, **where):
        return pltpu.make_async_remote_copy(src_ref=src, dst_ref=dst, send_sem=ss, recv_sem=rs,
                                            device_id=where, device_id_type=MESH)

    def w_copy(r):
        to = lax.rem(tpi + r, tp)
        return remote(wgt.at[pl.ds(pl.multiple_of(to * feat, feat), feat), :], w_in.at[r],
                      w_ss.at[r - 1], w_rs.at[r - 1], tp=to)

    def member(r):
        return lax.rem(y + r, inner)

    def a_copy(side, r, u):
        return remote(a_out.at[side, r - 1, u], a_in.at[side, r, u], a_ss.at[side, r - 1, u],
                      a_rs.at[side, r - 1, u], sp=z * inner + member(r))

    def b_copy(side, u):
        to = z + 1 if side == 0 else z - 1
        to = jnp.clip(to, 0, outer - 1)
        return remote(b_out.at[side, u], b_in.at[side, u], b_ss.at[side, u], b_rs.at[side, u],
                      sp=to * inner + y)

    def c_copy(side, r, u):
        return remote(c_out.at[side, r, u], c_in.at[side, r, u], c_ss.at[side, r - 1, u],
                      c_rs.at[side, r - 1, u], sp=z * inner + member(r))

    messages = own // group

    def d_copy(t, r, h, m):
        owner = lax.rem(y - r + inner, inner)
        first = pl.multiple_of((owner * own + m * group) * length, length)
        return remote(d_all.at[0, h, pl.ds(first, group * length), :],
                      d_all.at[t, h, pl.ds(first, group * length), :],
                      d_ss.at[t - 1, r, h, m], d_rs.at[t - 1, r, h, m], tp=lax.rem(tpi + t, tp))

    def d_wait(t, r, h, m):
        d_copy(t, r, h, m).wait_recv()

    def g_copy(r, h):
        to = lax.rem(spi + r, sp)
        return remote(g_out.at[h, to], g_in.at[h, r], g_ss.at[h, r - 1], g_rs.at[h, r - 1], sp=to)

    for r in range(1, tp):
        w_copy(r).start()
    w_in[0] = wgt[pl.ds(pl.multiple_of(tpi * feat, feat), feat), :]

    chunk = 4 * length
    total = batch * length

    def values(i, _):
        at = pl.ds(pl.multiple_of(i * chunk, chunk), chunk)
        val[at, :] = dot(hid[at, :], wgt[...]).astype(BF16)
        return 0

    mine = own * length // chunk if own * length % chunk == 0 else 0

    def values_of(r):
        lax.fori_loop(0, mine, lambda i, _: values(member(r) * mine + i, 0), 0)

    if mine:
        for r in range(1, inner):
            values_of(r)
    else:
        lax.fori_loop(0, total // chunk, values, 0)

    row = lax.broadcasted_iota(jnp.int32, (length, length), 0)
    col = lax.broadcasted_iota(jnp.int32, (length, length), 1)
    lower, upper = row >= col, row <= col
    ones_lower, ones_upper = jnp.where(lower, 1.0, 0.0), jnp.where(upper, 1.0, 0.0)
    sums = jnp.concatenate([ones_lower, ones_upper], 0).astype(BF16)
    strict = jnp.concatenate([jnp.where(row > col, 1.0, 0.0), jnp.where(row < col, 1.0, 0.0)], 0).astype(BF16)
    left = lax.broadcasted_iota(jnp.int32, (length, pack), 1) < dk
    tail_row = lax.broadcasted_iota(jnp.int32, (16, pack), 0)
    ones_tail = jnp.ones((16, dv), BF16)
    ones_dv = jnp.ones((16, dv), BF16)

    def both(matrix, x):
        high, low = split(x)
        out = dot(matrix, high) + dot(matrix, low)
        return jnp.where(left, out[:length], out[length:])

    def head_cols(ref, b, h):
        at = pl.ds(pl.multiple_of(b * length, length), length)
        return ref[at, pl.ds(pl.multiple_of(h * dv, dv), dv)]

    def twice(ref, b, h):
        x = ref[b, h].astype(F32)
        return jnp.concatenate([x, x], 1)

    def parts(b, h):
        c = both(sums, jnp.concatenate([fdec[b, h], bdec[b, h]], 1))
        cum[b, h] = c
        end = jnp.where(left[:1], c[length - 1:length], c[0:1])
        grow = (twice(qry, b, h) * jnp.exp(c)).astype(BF16)
        decay_key = (twice(key, b, h) * jnp.exp(end - c)).astype(BF16)
        state = dot(decay_key, head_cols(val, b, h), 0, 0)
        grad = dot(grow, head_cols(cot, b, h), 0, 0)
        high = end.astype(BF16).astype(F32)
        tail = jnp.where(tail_row == 0, high, jnp.where(tail_row == 1, end - high, 0.0))
        low = jnp.concatenate([state[:dk], grad[dk:], tail], 0).astype(BF16)
        up = jnp.concatenate([grad[:dk], state[dk:], tail], 0).astype(BF16)
        return low, up

    pair = 2 if units % 2 == 0 else 1

    def phase_one(i, _):
        todo = [(r, i * pair + n) for n in range(pair) for r in range(1, inner)]
        made = [parts(member(r) * own + lax.rem(u, own), u // own) for r, u in todo]
        for (r, u), sides in zip(todo, made):
            for side in range(2):
                a_out[side, r - 1, u] = sides[side]
        for r, u in todo:
            for side in range(2):
                a_copy(side, r, u).start()
        return 0

    lax.fori_loop(0, units // pair, phase_one, 0)
    if mine:
        values_of(0)

    def intra(b, h):
        c = cum[b, h]
        q_hat = (twice(qry, b, h) * jnp.exp(c)).astype(BF16)
        k_hat = (twice(key, b, h) * jnp.exp(-c)).astype(BF16)
        v, seed = head_cols(val, b, h), head_cols(cot, b, h)
        seed_scores = dot(seed, v, 1, 1)
        zero = jnp.zeros_like(q_hat)
        q_left, q_right = jnp.where(left, q_hat, zero), jnp.where(left, zero, q_hat)
        k_left, k_right = jnp.where(left, k_hat, zero), jnp.where(left, zero, k_hat)
        score = (jnp.where(lower, dot(q_left, k_hat, 1, 1), 0.0)
                 + jnp.where(upper, dot(q_right, k_hat, 1, 1), 0.0)).astype(BF16)
        seed_low = jnp.where(lower, seed_scores, 0.0).astype(BF16)
        seed_up = jnp.where(upper, seed_scores, 0.0).astype(BF16)
        intra_q[b, h] = dot(seed_low, k_left) + dot(seed_up, k_right)
        intra_k[b, h] = dot(seed_low, q_left, 0, 0) + dot(seed_up, q_right, 0, 0)
        intra_v[b, h] = dot(score, seed, 0, 0)

    def combine(side, u):
        @pl.when((z > 0) if side == 0 else (z < outer - 1))
        def _():
            b_copy(side, u).wait_recv()

        first = (z == 0) if side == 0 else (z == outer - 1)

        @pl.when(first)
        def _():
            b_in[side, u] = jnp.zeros((pack, dv), BF16)

        for r in range(1, inner):
            a_copy(side, r, u).wait_recv()
        running = b_in[side, u].astype(F32)
        order = range(inner) if side == 0 else range(inner - 1, -1, -1)
        for person in order:
            r = lax.rem(person - y + inner, inner)
            source = lax.rem(y - person + inner, inner)
            c_out[side, r, u] = running.astype(BF16)
            message = a_in[side, source, u]
            factor = jnp.exp(dot(message[pack:], ones_tail, 0, 0))
            running = factor * running + message[:pack].astype(F32)
        b_out[side, u] = running.astype(BF16)

        @pl.when((z < outer - 1) if side == 0 else (z > 0))
        def _():
            b_copy(side, u).start()

        c_in[side, 0, u] = c_out[side, 0, u]
        for r in range(1, inner):
            c_copy(side, r, u).start()

    def finish(r, u, h, step):
        b = lax.rem(y - r + inner, inner) * own + step
        low, up = c_in[0, r, u], c_in[1, r, u]
        state = jnp.concatenate([low[:dk], up[dk:]], 0)
        grad = jnp.concatenate([up[:dk], low[dk:]], 0)
        c = cum[b, h]
        end = jnp.where(left[:1], c[length - 1:length], c[0:1])
        grow, shrink, to_end = jnp.exp(c), jnp.exp(-c), jnp.exp(end - c)
        q, k = twice(qry, b, h), twice(key, b, h)
        v, seed = head_cols(val, b, h), head_cols(cot, b, h)
        cross = dot(seed, state, 1, 1)
        dq = grow * (intra_q[b, h] + cross)
        dk_ = shrink * intra_k[b, h] + to_end * dot(v, grad, 1, 1)
        dv_ = intra_v[b, h] + dot((k * to_end).astype(BF16), grad)
        g = q * dq - k * dk_
        pair = (state.astype(F32) * grad.astype(F32)).astype(BF16)
        start = (jnp.sum(q * grow * cross, axis=0, keepdims=True)
                 + jnp.exp(end) * dot(ones_dv, pair, 1, 1)[:1])
        decay_grad = start - both(strict, g)
        o_qk[b, h] = jnp.concatenate([dq[:, :dk] + dq[:, dk:], dk_[:, :dk] + dk_[:, dk:]], 1).astype(BF16)
        o_fb[b, h] = decay_grad
        d_all[0, h, pl.ds(pl.multiple_of(b * length, length), length), :] = dv_.astype(BF16)

    def weight_term(h):
        full = dot(d_all[0, h], hid[...], 0, 0)
        for p in range(sp):
            g_out[h, p] = full[:, p * rows_sp:(p + 1) * rows_sp].astype(BF16)
        for r in range(1, sp):
            g_copy(r, h).start()

    delay = (outer - 1) * LAG + 1 + EXTRA

    def phase_two(s, _):
        for side in range(2):
            at = s - 1 - (z if side == 0 else outer - 1 - z) * LAG

            @pl.when((at >= 0) & (at < units))
            def _():
                combine(side, at)

        @pl.when(s < units)
        def _():
            h, step = s // own, lax.rem(s, own)
            low, up = parts(y * own + step, h)
            a_in[0, 0, s] = low
            a_in[1, 0, s] = up
            for r in range(inner):
                intra(member(r) * own + step, h)

        last = s - delay

        @pl.when(last >= 0)
        def _():
            h, step = last // own, lax.rem(last, own)
            for side in range(2):
                for r in range(1, inner):
                    c_copy(side, r, last).wait_recv()
            for r in range(inner):
                finish(r, last, h, step)

            @pl.when(lax.rem(step + 1, group) == 0)
            def _():
                m = step // group
                for r in range(inner):
                    for t in range(1, tp):
                        d_copy(t, r, h, m).start()

            @pl.when(step == own - 1)
            def _():
                weight_term(h)
        return 0

    lax.fori_loop(0, units + delay, phase_two, 0)

    for t in range(1, tp):
        w_copy(t).wait_recv()
        for r in range(inner):
            for h in range(heads):
                for m in range(messages):
                    d_wait(t, r, h, m)

    def features(i, _):
        at = pl.ds(pl.multiple_of(i * chunk, chunk), chunk)
        acc = jnp.zeros((chunk, feat), F32)
        for t in range(tp):
            for h in range(heads):
                acc = acc + dot(d_all[t, h, at, :], w_in[t, :, h * dv:(h + 1) * dv], 1, 1)
        o_h[at, :] = acc.astype(BF16)
        return 0

    lax.fori_loop(0, total // chunk, features, 0)

    for h in range(heads):
        acc = g_out[h, spi].astype(F32)
        for r in range(1, sp):
            g_copy(r, h).wait_recv()
            acc = acc + g_in[h, r].astype(F32)
        o_w[:, h * dv:(h + 1) * dv] = acc.T

    for r in range(1, tp):
        w_copy(r).wait_send()
    for h in range(heads):
        for r in range(1, sp):
            g_copy(r, h).wait_send()
        for m in range(messages):
            for t in range(1, tp):
                for r in range(inner):
                    d_copy(t, r, h, m).wait_send()

    def drain(u, _):
        for side in range(2):
            for r in range(1, inner):
                a_copy(side, r, u).wait_send()
                c_copy(side, r, u).wait_send()

            @pl.when((z < outer - 1) if side == 0 else (z > 0))
            def _():
                b_copy(side, u).wait_send()
        return 0

    lax.fori_loop(0, units, drain, 0)


def d_group(own):
    return 4 if own % 4 == 0 else 1


def shards(sp, tp, hidden, value_weight, queries, key_vectors, forward_decay, backward_decay, cotangent):
    batch, length, width = hidden.shape
    heads, dk = queries.shape[1], queries.shape[3]
    cols = value_weight.shape[1]
    dv = cols // heads
    outer, inner, own, units = plan(sp, batch, heads)
    pack, rows, feat, rows_sp = 2 * dk, batch * length, width // tp, width // sp
    group = d_group(own)
    dims = (sp, tp, batch, heads, length, dk, dv, width)
    vmem, dma = pltpu.VMEM, pltpu.SemaphoreType.DMA
    peers = max(inner - 1, 1)
    scratch = [
        vmem((rows, cols), BF16),
        vmem((batch, heads, length, pack), F32),
        vmem((batch, heads, length, pack), F32),
        vmem((batch, heads, length, pack), F32),
        vmem((batch, heads, length, dv), F32),
        vmem((2, peers, units, pack + 16, dv), BF16),
        vmem((2, inner, units, pack + 16, dv), BF16),
        vmem((2, units, pack, dv), BF16),
        vmem((2, units, pack, dv), BF16),
        vmem((2, inner, units, pack, dv), BF16),
        vmem((2, inner, units, pack, dv), BF16),
        vmem((tp, heads, rows, dv), BF16),
        vmem((tp, feat, cols), BF16),
        vmem((heads, sp, dv, rows_sp), BF16),
        vmem((heads, sp, dv, rows_sp), BF16),
        dma((2, peers, units)), dma((2, peers, units)),
        dma((2, units)), dma((2, units)),
        dma((2, peers, units)), dma((2, peers, units)),
        dma((tp - 1, inner, heads, own // group)), dma((tp - 1, inner, heads, own // group)),
        dma((tp - 1,)), dma((tp - 1,)),
        dma((heads, sp - 1)), dma((heads, sp - 1)),
    ]
    whole = pl.BlockSpec(memory_space=vmem)
    outs = pl.pallas_call(
        functools.partial(kernel, dims),
        out_shape=(
            jax.ShapeDtypeStruct((batch, heads, length, pack), BF16),
            jax.ShapeDtypeStruct((batch, heads, length, pack), F32),
            jax.ShapeDtypeStruct((rows, feat), BF16),
            jax.ShapeDtypeStruct((rows_sp, cols), F32),
        ),
        in_specs=[whole] * 7,
        out_specs=(whole,) * 4,
        scratch_shapes=scratch,
        compiler_params=pltpu.CompilerParams(
            collective_id=0, has_side_effects=True, vmem_limit_bytes=60 * 1024 * 1024
        ),
    )(hidden.reshape(rows, width), value_weight, queries, key_vectors, forward_decay, backward_decay,
      cotangent.reshape(rows, cols))
    near, decays = outs[0], outs[1]
    return (near[..., :dk], near[..., dk:], decays[..., :dk], decays[..., dk:],
            outs[2].reshape(batch, length, feat), outs[3])


def solution(mesh):
    heads = P(None, "tp", "sp", None)
    return jax.shard_map(
        functools.partial(shards, mesh.shape["sp"], mesh.shape["tp"]),
        mesh=mesh,
        in_specs=(P(None, "sp", None), P(None, "tp"), heads, heads, heads, heads, P(None, "sp", "tp")),
        out_specs=(heads, heads, heads, heads, P(None, "sp", "tp"), P("sp", "tp")),
        check_vma=False,
    )
```

profile of v0, /device:TPU:1, one launch (start us, length us, event | category | flops | bytes accessed | tf_op | source)
XLA Modules:
  0.0 72.9 jit_solution(1918216270705898605)
XLA Ops:
  0.6 67.7 %shard_map.118 = (bf16[16,1,64,128]{3,2,1,0:T(8,128)(2,1)}, f32[16,1,64,128]{3,2,1,0:T(8,128)}, bf16[1024,128]{1,0:T(8,128)(2,1)}, f32[64,128]{1,0:T(8,128)}) custom-call(bf16[1024,1024]{1,0:T(8,128)(2,1)} %bitcast.3, bf16[1024,128]{1,0:T(8,128)(2,1)} %wgt.1, bf16[16,1,64,64]{3,2,1,0:T(8,128)(2,1)} %qry.1, bf16[16,1,64,64]{3,2,1,0:T(8,128)(2,1)} %key.1, ...), custom_call_target="tpu_custom_call" | custom-call | tf_op jit(solution)/shard_map/pallas_call | solution.py:384
  68.3 0.0 copy-start
  68.3 0.0 copy-start.1
  68.3 0.0 copy-start.2
  68.4 2.4 %fusion = (f32[16,1,64,64]{3,2,1,0:T(8,128)}, f32[16,1,64,64]{3,2,1,0:T(8,128)}) fusion(f32[16,1,64,128]{3,2,1,0:T(8,128)} %get-tuple-element.11), kind=kLoop, calls=%fused_computation | loop fusion | bytes 1048576 | tf_op jit(solution)/shard_map/slice | solution.py:401
  70.7 0.0 copy-done
  70.7 0.9 %fusion.1 = (bf16[16,1,64,64]{3,2,1,0:T(8,128)(2,1)}, bf16[16,1,64,64]{3,2,1,0:T(8,128)(2,1)}) fusion(bf16[16,1,64,128]{3,2,1,0:T(8,128)(2,1)S(1)} %copy-done), kind=kLoop, calls=%fused_computation.1 | loop fusion | bytes 524288 | tf_op jit(solution)/shard_map/slice | solution.py:401
  71.6 0.0 copy-done.1
  71.6 0.7 copy.15
  72.3 0.0 copy-done.2
  72.3 0.6 copy.16
Async XLA Ops:
  68.3 2.4 %copy-start = (bf16[16,1,64,128]{3,2,1,0:T(8,128)(2,1)S(1)}, bf16[16,1,64,128]{3,2,1,0:T(8,128)(2,1)}, u32[]{:S(2)}) copy-start(bf16[16,1,64,128]{3,2,1,0:T(8,128)(2,1)} %get-tuple-element.10) | copy-start | bytes 786436
  68.3 3.3 %copy-start.1 = (bf16[1024,128]{1,0:T(8,128)(2,1)S(1)}, bf16[1024,128]{1,0:T(8,128)(2,1)}, u32[]{:S(2)}) copy-start(bf16[1024,128]{1,0:T(8,128)(2,1)} %get-tuple-element.12) | copy-start | bytes 786436
  68.3 4.0 %copy-start.2 = (f32[64,128]{1,0:T(8,128)S(1)}, f32[64,128]{1,0:T(8,128)}, u32[]{:S(2)}) copy-start(f32[64,128]{1,0:T(8,128)} %get-tuple-element.29) | copy-start | bytes 98308
where the time goes:
time: 73.1 us; the launch traced here: 72.9 us
  Pallas kernels  67.7 us (93%)
  local copies, waits for them, and re-layouts  4.58 us (6%)
    pallas_call x1, Pallas kernels, shards(): pl.pallas_call(functools.partial(kernel, dims), out_shape=(jax.ShapeDtype...  67.7 us
    slice x1, local copies, waits for them, and re-layouts, shards(): decays[..., dk:]  2.37 us

commit v1 on v0

--- a/solution.py
+++ b/solution.py
@@ -30,7 +30,7 @@
 
 
 def kernel(dims, hid, wgt, qry, key, fdec, bdec, cot,
-           o_qk, o_fb, o_h, o_w,
+           o_q, o_k, o_f, o_b, o_h, o_w,
            val, cum, intra_q, intra_k, intra_v,
            a_out, a_in, b_out, b_in, c_out, c_in, d_all, w_in, g_out, g_in,
            a_ss, a_rs, b_ss, b_rs, c_ss, c_rs, d_ss, d_rs, w_ss, w_rs, g_ss, g_rs):
@@ -238,8 +238,10 @@
         start = (jnp.sum(q * grow * cross, axis=0, keepdims=True)
                  + jnp.exp(end) * dot(ones_dv, pair, 1, 1)[:1])
         decay_grad = start - both(strict, g)
-        o_qk[b, h] = jnp.concatenate([dq[:, :dk] + dq[:, dk:], dk_[:, :dk] + dk_[:, dk:]], 1).astype(BF16)
-        o_fb[b, h] = decay_grad
+        o_q[b, h] = (dq[:, :dk] + dq[:, dk:]).astype(BF16)
+        o_k[b, h] = (dk_[:, :dk] + dk_[:, dk:]).astype(BF16)
+        o_f[b, h] = decay_grad[:, :dk]
+        o_b[b, h] = decay_grad[:, dk:]
         d_all[0, h, pl.ds(pl.multiple_of(b * length, length), length), :] = dv_.astype(BF16)
 
     def weight_term(h):
@@ -384,22 +386,45 @@
     outs = pl.pallas_call(
         functools.partial(kernel, dims),
         out_shape=(
-            jax.ShapeDtypeStruct((batch, heads, length, pack), BF16),
-            jax.ShapeDtypeStruct((batch, heads, length, pack), F32),
-            jax.ShapeDtypeStruct((rows, feat), BF16),
-            jax.ShapeDtypeStruct((rows_sp, cols), F32),
+            vmem((batch, heads, length, dk), BF16),
+            vmem((batch, heads, length, dk), BF16),
+            vmem((batch, heads, length, dk), F32),
+            vmem((batch, heads, length, dk), F32),
+            vmem((rows, feat), BF16),
+            vmem((rows_sp, cols), F32),
         ),
         in_specs=[whole] * 7,
-        out_specs=(whole,) * 4,
+        out_specs=(whole,) * 6,
         scratch_shapes=scratch,
         compiler_params=pltpu.CompilerParams(
-            collective_id=0, has_side_effects=True, vmem_limit_bytes=60 * 1024 * 1024
+            collective_id=0, has_side_effects=True, vmem_limit_bytes=40 * 1024 * 1024
         ),
     )(hidden.reshape(rows, width), value_weight, queries, key_vectors, forward_decay, backward_decay,
       cotangent.reshape(rows, cols))
-    near, decays = outs[0], outs[1]
-    return (near[..., :dk], near[..., dk:], decays[..., :dk], decays[..., dk:],
-            outs[2].reshape(batch, length, feat), outs[3])
+    outs = store(outs)
+    return outs[:4] + (outs[4].reshape(batch, length, feat), outs[5])
+
+
+def store_kernel(*refs):
+    n = len(refs) // 2
+    sems = refs[-1]
+    copies = [pltpu.make_async_copy(refs[i], refs[n + i], sems.at[i]) for i in range(n)]
+    for copy in copies:
+        copy.start()
+    for copy in copies:
+        copy.wait()
+
+
+def store(arrays):
+    n = len(arrays)
+    return pl.pallas_call(
+        store_kernel,
+        out_shape=tuple(jax.ShapeDtypeStruct(a.shape, a.dtype) for a in arrays),
+        in_specs=[pl.BlockSpec(memory_space=pltpu.VMEM)] * n,
+        out_specs=(pl.BlockSpec(memory_space=pl.ANY),) * n,
+        scratch_shapes=[pltpu.SemaphoreType.DMA((n,))],
+        compiler_params=pltpu.CompilerParams(has_side_effects=True, vmem_limit_bytes=1024 * 1024),
+    )(*arrays)
 
 
 def solution(mesh):

time: 73.1 us -> 74.4 us (1.018)
  local copies, waits for them, and re-layouts: 4.58 us -> 7.46 us
  Pallas kernels: 67.7 us -> 65.9 us
    unnamed x8 -> x14, local copies, waits for them, and re-layouts: 1.33 us -> 7.46 us
    slice x2 -> x0, local copies, waits for them, and re-layouts: 3.25 us -> none  [the longest x1 2.37 us: shards(): decays[..., dk:]]
    pallas_call x1 -> x2, Pallas kernels: 67.7 us -> 65.9 us  [the longest x1 64.6 us: shards(): pl.pallas_call(functools.partial(kernel, dims), out_shape=(vmem((batch, h...]
where the time goes in v1:
time: 74.4 us; the launch traced here: 74 us
  Pallas kernels  65.9 us (89%)
  local copies, waits for them, and re-layouts  7.46 us (10%)
    pallas_call x1, Pallas kernels, shards(): pl.pallas_call(functools.partial(kernel, dims), out_shape=(vmem((batch, h...  64.6 us
    unnamed x14, local copies, waits for them, and re-layouts  7.46 us

profile of v1, /device:TPU:1, one launch (start us, length us, event | category | flops | bytes accessed | tf_op | source)
XLA Modules:
  0.0 74.0 jit_solution(17682533856579117881)
XLA Ops:
  0.6 0.0 copy-start
  0.6 1.6 %copy-done = bf16[16,64,1024]{2,1,0:T(8,128)(2,1)S(1)} copy-done((bf16[16,64,1024]{2,1,0:T(8,128)(2,1)S(1)}, bf16[16,64,1024]{2,1,0:T(8,128)(2,1)}, u32[]{:S(2)}) %copy-start) | copy-done | bytes 2097176
  2.2 0.0 copy-start.1
  2.2 1.0 %copy-done.1 = f32[16,1,64,64]{3,2,1,0:T(8,128)S(1)} copy-done((f32[16,1,64,64]{3,2,1,0:T(8,128)S(1)}, f32[16,1,64,64]{3,2,1,0:T(8,128)}, u32[]{:S(2)}) %copy-start.1) | copy-done | bytes 262168
  3.3 0.0 copy-start.2
  3.3 1.0 %copy-done.2 = f32[16,1,64,64]{3,2,1,0:T(8,128)S(1)} copy-done((f32[16,1,64,64]{3,2,1,0:T(8,128)S(1)}, f32[16,1,64,64]{3,2,1,0:T(8,128)}, u32[]{:S(2)}) %copy-start.2) | copy-done | bytes 262168
  4.3 0.0 copy-start.3
  4.3 0.9 %copy-done.3 = bf16[1024,128]{1,0:T(8,128)(2,1)S(1)} copy-done((bf16[1024,128]{1,0:T(8,128)(2,1)S(1)}, bf16[1024,128]{1,0:T(8,128)(2,1)}, u32[]{:S(2)}) %copy-start.3) | copy-done | bytes 262168
  5.3 0.0 copy-start.4
  5.3 0.9 %copy-done.4 = bf16[16,1,64,64]{3,2,1,0:T(8,128)(2,1)S(1)} copy-done((bf16[16,1,64,64]{3,2,1,0:T(8,128)(2,1)S(1)}, bf16[16,1,64,64]{3,2,1,0:T(8,128)(2,1)}, u32[]{:S(2)}) %copy-start.4) | copy-done | bytes 131096
  6.2 0.0 copy-start.5
  6.2 0.9 %copy-done.5 = bf16[16,1,64,64]{3,2,1,0:T(8,128)(2,1)S(1)} copy-done((bf16[16,1,64,64]{3,2,1,0:T(8,128)(2,1)S(1)}, bf16[16,1,64,64]{3,2,1,0:T(8,128)(2,1)}, u32[]{:S(2)}) %copy-start.5) | copy-done | bytes 131096
  7.2 0.0 copy-start.6
  7.2 0.9 %copy-done.6 = bf16[16,64,128]{2,1,0:T(8,128)(2,1)S(1)} copy-done((bf16[16,64,128]{2,1,0:T(8,128)(2,1)S(1)}, bf16[16,64,128]{2,1,0:T(8,128)(2,1)}, u32[]{:S(2)}) %copy-start.6) | copy-done | bytes 262168
  8.1 64.6 %shard_map.118 = (bf16[16,1,64,64]{3,2,1,0:T(8,128)(2,1)S(1)}, bf16[16,1,64,64]{3,2,1,0:T(8,128)(2,1)S(1)}, f32[16,1,64,64]{3,2,1,0:T(8,128)S(1)}, f32[16,1,64,6...) custom-call(bf16[1024,1024]{1,0:T(8,128)(2,1)S(1)} %bitcast.3, ...), custom_call_target="tpu_custom_call" | custom-call | tf_op jit(solution)/shard_map/pallas_call | solution.py:386
  72.8 1.3 %shard_map.119 = (bf16[16,1,64,64]{3,2,1,0:T(8,128)(2,1)}, bf16[16,1,64,64]{3,2,1,0:T(8,128)(2,1)}, f32[16,1,64,64]{3,2,1,0:T(8,128)}, f32[16,1,64,64]{3,2,1,0:T...) custom-call(bf16[16,1,64,64]{3,2,1,0:T(8,128)(2,1)S(1)} %get-tuple-element.18.refs_0_, ...), custom_call_target="tpu_custom_call" | custom-call | tf_op jit(solution)/shard_map/pallas_call | solution.py:420
Async XLA Ops:
  0.6 1.6 %copy-start = (bf16[16,64,1024]{2,1,0:T(8,128)(2,1)S(1)}, bf16[16,64,1024]{2,1,0:T(8,128)(2,1)}, u32[]{:S(2)}) copy-start(bf16[16,64,1024]{2,1,0:T(8,128)(2,1)} %param.7) | copy-start | bytes 6291460
  2.2 1.0 %copy-start.1 = (f32[16,1,64,64]{3,2,1,0:T(8,128)S(1)}, f32[16,1,64,64]{3,2,1,0:T(8,128)}, u32[]{:S(2)}) copy-start(f32[16,1,64,64]{3,2,1,0:T(8,128)} %fdec.1) | copy-start | bytes 786436
  3.3 1.0 %copy-start.2 = (f32[16,1,64,64]{3,2,1,0:T(8,128)S(1)}, f32[16,1,64,64]{3,2,1,0:T(8,128)}, u32[]{:S(2)}) copy-start(f32[16,1,64,64]{3,2,1,0:T(8,128)} %bdec.1) | copy-start | bytes 786436
  4.3 0.9 %copy-start.3 = (bf16[1024,128]{1,0:T(8,128)(2,1)S(1)}, bf16[1024,128]{1,0:T(8,128)(2,1)}, u32[]{:S(2)}) copy-start(bf16[1024,128]{1,0:T(8,128)(2,1)} %wgt.1) | copy-start | bytes 786436
  5.3 0.9 %copy-start.4 = (bf16[16,1,64,64]{3,2,1,0:T(8,128)(2,1)S(1)}, bf16[16,1,64,64]{3,2,1,0:T(8,128)(2,1)}, u32[]{:S(2)}) copy-start(bf16[16,1,64,64]{3,2,1,0:T(8,128)(2,1)} %qry.1) | copy-start | bytes 393220
  6.2 0.9 %copy-start.5 = (bf16[16,1,64,64]{3,2,1,0:T(8,128)(2,1)S(1)}, bf16[16,1,64,64]{3,2,1,0:T(8,128)(2,1)}, u32[]{:S(2)}) copy-start(bf16[16,1,64,64]{3,2,1,0:T(8,128)(2,1)} %key.1) | copy-start | bytes 393220
  7.2 0.9 %copy-start.6 = (bf16[16,64,128]{2,1,0:T(8,128)(2,1)S(1)}, bf16[16,64,128]{2,1,0:T(8,128)(2,1)}, u32[]{:S(2)}) copy-start(bf16[16,64,128]{2,1,0:T(8,128)(2,1)} %param.13) | copy-start | bytes 786436

commit v2 on v0

v2 whole, which is shorter than its diff:
```python
import functools

import jax
import jax.numpy as jnp
from jax import lax
from jax.experimental import pallas as pl
from jax.experimental.pallas import tpu as pltpu
from jax.sharding import PartitionSpec as P

F32, BF16 = jnp.float32, jnp.bfloat16
MESH = pl.DeviceIdType.MESH
CORES = 2
INNER = 4


def dot(a, b, ca=1, cb=0):
    return lax.dot_general(a, b, (((ca,), (cb,)), ((), ())), preferred_element_type=F32)


def halves(x):
    high = x.astype(BF16)
    return jnp.concatenate([high, (x - high.astype(F32)).astype(BF16)], 0)


def kernel(dims, hid, wgt, qry, key, fdec, bdec, cot,
           o_q, o_k, o_f, o_b, o_h, o_w,
           hid_v, wgt_v, q_v, k_v, f_v, b_v, cot_v,
           val, cum, q_hats, k_ends, intra_q, intra_k, intra_v,
           a_out, a_in, e_out, e_in, local, b_out, b_in, c_out, c_in,
           d_all, w_in, w_acc, g_out, g_in,
           i_s, h_s, a_ss, a_rs, e_ss, e_rs, b_ss, b_rs, c_ss, c_rs,
           d_ss, d_rs, p_ss, p_rs, f_ss, f_rs, w_ss, w_rs, g_ss, g_rs):
    sp, tp, batch, length, dk, dv, width = dims
    inner, outer, own, xs = INNER, sp // INNER, batch // INNER, tp // CORES
    pack, feat, rows_sp, group = 2 * dk, width // tp, width // sp, INNER * length
    spi, tpi = lax.axis_index("sp"), lax.axis_index("tp")
    z, y = spi // inner, lax.rem(spi, inner)
    x, core = tpi // CORES, lax.rem(tpi, CORES)

    barrier = pltpu.get_barrier_semaphore()
    for r in range(1, sp):
        pl.semaphore_signal(barrier, inc=1, device_id={"sp": lax.rem(spi + r, sp)}, device_id_type=MESH)
    for r in range(1, tp):
        pl.semaphore_signal(barrier, inc=1, device_id={"tp": lax.rem(tpi + r, tp)}, device_id_type=MESH)

    def owner(r):
        return lax.rem(y + r, inner)

    def batch_of(r, u):
        return owner(r) * own + u

    def slot(r, u):
        return u * inner + r

    def rows(r, u, count=1):
        return pl.ds(pl.multiple_of(slot(r, u) * length, length), count * length)

    small = [pltpu.make_async_copy(src, dst, i_s.at[i]) for i, (src, dst) in enumerate(
        ((fdec, f_v), (bdec, b_v), (qry, q_v), (cot, cot_v), (wgt, wgt_v), (key, k_v)))]

    def load_hidden(r, u):
        return pltpu.make_async_copy(hid.at[batch_of(r, u)], hid_v.at[rows(r, u)], h_s.at[slot(r, u)])

    for copy in small[:5]:
        copy.start()
    for u in range(own):
        for r in range(inner):
            load_hidden(r, u).start()
        if u == 0:
            small[5].start()

    def remote(src, dst, ss, rs, **where):
        return pltpu.make_async_remote_copy(src_ref=src, dst_ref=dst, send_sem=ss, recv_sem=rs,
                                            device_id=where, device_id_type=MESH)

    def w_copy(r):
        to = lax.rem(tpi + r, tp)
        return remote(wgt_v.at[pl.ds(pl.multiple_of(to * feat, feat), feat), :], w_in.at[tpi],
                      w_ss.at[r - 1], w_rs.at[r - 1], tp=to)

    def a_copy(kind, r, u):
        return remote(a_out.at[kind, r - 1, u], a_in.at[kind, r, u], a_ss.at[kind, r - 1, u],
                      a_rs.at[kind, r - 1, u], sp=z * inner + owner(r))

    def e_copy(r):
        to = lax.rem(spi + r, sp)
        return remote(e_out.at[lax.rem(to, inner)], e_in.at[r], e_ss.at[r - 1], e_rs.at[r - 1], sp=to)

    def b_copy(side, r, u):
        to = jnp.clip(z + r if side == 0 else z - r, 0, outer - 1)
        return remote(b_out.at[side, u], b_in.at[side, r - 1, u], b_ss.at[side, r - 1, u],
                      b_rs.at[side, r - 1, u], sp=to * inner + y)

    def above(r):
        return z + r < outer

    def below(r):
        return z >= r

    def c_copy(side, r, u):
        return remote(c_out.at[side, r, u], c_in.at[side, r - 1, u], c_ss.at[side, r - 1, u],
                      c_rs.at[side, r - 1, u], sp=z * inner + lax.rem(y - r + inner, inner))

    def part_rows(u, part):
        return rows(0, u) if part == 0 else rows(1, u, inner - 1)

    def d_copy(r, u, part):
        at = part_rows(u, part)
        return remote(d_all.at[tpi, at], d_all.at[tpi, at], d_ss.at[r - 1, u, part],
                      d_rs.at[r - 1, u, part], tp=lax.rem(x + r, xs) * CORES + core)

    mate = x * CORES + 1 - core

    def p_copy(u, part):
        at = part_rows(u, part)
        return remote(d_all.at[tpi, at], d_all.at[tpi, at], p_ss.at[u, part], p_rs.at[u, part], tp=mate)

    def f_copy(r, u):
        source = lax.rem(x - r + xs, xs) * CORES + core
        at = rows(0, u, inner)
        return remote(d_all.at[source, at], d_all.at[source, at], f_ss.at[r - 1, u], f_rs.at[r - 1, u], tp=mate)

    def g_copy(r):
        to = lax.rem(spi + r, sp)
        return remote(g_out.at[to], g_in.at[r - 1], g_ss.at[r - 1], g_rs.at[r - 1], sp=to)

    row = lax.broadcasted_iota(jnp.int32, (length, length), 0)
    col = lax.broadcasted_iota(jnp.int32, (length, length), 1)
    lower, upper = row >= col, row <= col

    def matrix(first, second):
        both = jnp.concatenate([jnp.where(first, 1.0, 0.0), jnp.where(second, 1.0, 0.0)], 0)
        return jnp.concatenate([both, both], 1).astype(BF16)

    sums, strict = matrix(lower, upper), matrix(row > col, row < col)
    left = lax.broadcasted_iota(jnp.int32, (length, pack), 1) < dk
    left_tall = lax.broadcasted_iota(jnp.int32, (dv, pack), 1) < dk

    def directed(tri, blocks):
        made = []
        for i in range(0, len(blocks), 2):
            pair = blocks[i:i + 2]
            out = dot(tri, halves(jnp.concatenate(pair, 1) if len(pair) > 1 else pair[0]))
            for n in range(len(pair)):
                part = out[:, n * pack:(n + 1) * pack]
                made.append(jnp.where(left, part[:length], part[length:]))
        return made

    def twice(ref, b):
        v = ref[b].astype(F32)
        return jnp.concatenate([v, v], 1)

    def ends(c):
        return jnp.where(left[:1], c[length - 1:length], c[0:1])

    for side in range(2):
        for r in range(1, outer):
            @pl.when(jnp.logical_not(below(r) if side == 0 else above(r)))
            def _():
                b_in[side, r - 1] = jnp.zeros((own, dv, pack), BF16)

    for copy in small[:2]:
        copy.wait()

    def decays(u, _):
        blocks = [jnp.concatenate([f_v[batch_of(r, u)], b_v[batch_of(r, u)]], 1) for r in range(inner)]
        made = directed(sums, blocks)
        for r in range(inner):
            cum[slot(r, u)] = made[r]
        for r in range(inner):
            e_out[owner(r), pl.ds(u, 1), :] = ends(made[r])
        return 0

    lax.fori_loop(0, own, decays, 0)

    def grads(todo):
        hats = [(twice(q_v, batch_of(r, u)) * jnp.exp(cum[slot(r, u)])).astype(BF16) for r, u in todo]
        made = [dot(cot_v[batch_of(r, u)], hat, 0, 0).astype(BF16) for (r, u), hat in zip(todo, hats)]
        return hats, made

    def states(todo):
        keys = []
        for r, u in todo:
            c = cum[slot(r, u)]
            keys.append((twice(k_v, batch_of(r, u)) * jnp.exp(ends(c) - c)).astype(BF16))
        made = [dot(val[rows(r, u)], k_end, 0, 0).astype(BF16) for (r, u), k_end in zip(todo, keys)]
        return keys, made

    def place(kind, r, u, value):
        if r == 0:
            a_in[kind, 0, u] = value
        else:
            a_out[kind, r - 1, u] = value

    def emit(kind, todo):
        kept, made = (grads if kind == 0 else states)(todo)
        keep = q_hats if kind == 0 else k_ends
        for (r, u), value, block in zip(todo, kept, made):
            keep[slot(r, u)] = value
            place(kind, r, u, block)

    def values(u):
        at = rows(0, u, inner)
        val[at] = dot(hid_v[at], wgt_v[...]).astype(BF16)

    for copy in small[2:4]:
        copy.wait()

    bunch = 2 if own % 2 == 0 else 1
    for first in range(0, own, bunch):
        todo = [(r, first + n) for n in range(bunch) for r in range(1, inner)]
        emit(0, todo)
        if first == 0:
            pl.semaphore_wait(barrier, sp + tp - 2)
            for r in range(1, sp):
                e_copy(r).start()
        for r, u in todo:
            a_copy(0, r, u).start()
        if first == 0:
            for copy in small[4:]:
                copy.wait()
            for r in range(1, tp):
                w_copy(r).start()
            w_in[tpi] = wgt_v[pl.ds(pl.multiple_of(tpi * feat, feat), feat), :]
            e_in[0] = e_out[y]
        for n in range(bunch):
            for r in range(inner):
                load_hidden(r, first + n).wait()
            values(first + n)
        emit(1, todo)
        for r, u in todo:
            a_copy(1, r, u).start()

    mine = [(0, u) for u in range(own)]
    emit(0, mine)
    emit(1, mine)
    w_acc[...] = jnp.zeros((dv, width), F32)
    for r in range(1, sp):
        e_copy(r).wait_recv()

    def ending(plane, person, u):
        source = lax.rem(spi - (plane * inner + person) + sp, sp)
        return e_in[source, pl.ds(u, 1), :]

    people = (tuple(range(inner)), tuple(range(inner - 1, -1, -1)))

    def offset(person):
        return lax.rem(y - person + inner, inner)

    def combine_plane(u):
        for kind in range(2):
            for r in range(1, inner):
                a_copy(kind, r, u).wait_recv()
        for side in range(2):
            running = jnp.zeros((dv, pack), F32)
            for n, person in enumerate(people[side]):
                grad, state = a_in[0, offset(person), u], a_in[1, offset(person), u]
                block = jnp.where(left_tall, state, grad) if side == 0 else jnp.where(left_tall, grad, state)
                if n == 0:
                    running = block.astype(F32)
                else:
                    local[side, person, u] = running
                    running = jnp.exp(ending(z, person, u)) * running + block.astype(F32)
            b_out[side, u] = running.astype(BF16)
        for side in range(2):
            for r in range(1, outer):
                @pl.when(above(r) if side == 0 else below(r))
                def _():
                    b_copy(side, r, u).start()

    def combine_all(u):
        for side in range(2):
            for r in range(1, outer):
                @pl.when(below(r) if side == 0 else above(r))
                def _():
                    b_copy(side, r, u).wait_recv()
        for side in range(2):
            carried = b_in[side, 0, u].astype(F32)
            passed = jnp.zeros((1, pack), F32)
            for r in range(2, outer):
                plane = lax.rem(z - r + 1 + outer, outer) if side == 0 else lax.rem(z + r - 1, outer)
                for person in range(inner):
                    passed = passed + ending(plane, person, u)
                carried = carried + jnp.exp(passed) * b_in[side, r - 1, u].astype(F32)
            passed = jnp.zeros((1, pack), F32)
            for n, person in enumerate(people[side]):
                if n == 0:
                    c_out[side, offset(person), u] = carried.astype(BF16)
                else:
                    out = jnp.exp(passed) * carried + local[side, person, u]
                    c_out[side, offset(person), u] = out.astype(BF16)
                passed = passed + ending(z, person, u)
        for side in range(2):
            for r in range(1, inner):
                c_copy(side, r, u).start()

    def intra(todo):
        made = []
        for r, u in todo:
            b, s = batch_of(r, u), slot(r, u)
            q_hat = q_hats[s]
            k_hat = (twice(k_v, b) * jnp.exp(-cum[s])).astype(BF16)
            v, seed = val[rows(r, u)], cot_v[b]
            seed_scores = dot(seed, v, 1, 1)
            zero = jnp.zeros_like(q_hat)
            q_left, q_right = jnp.where(left, q_hat, zero), jnp.where(left, zero, q_hat)
            k_left, k_right = jnp.where(left, k_hat, zero), jnp.where(left, zero, k_hat)
            score = (jnp.where(lower, dot(q_left, k_hat, 1, 1), 0.0)
                     + jnp.where(upper, dot(q_right, k_hat, 1, 1), 0.0)).astype(BF16)
            seed_low = jnp.where(lower, seed_scores, 0.0).astype(BF16)
            seed_up = jnp.where(upper, seed_scores, 0.0).astype(BF16)
            made.append((dot(seed_low, k_left) + dot(seed_up, k_right),
                         dot(seed_low, q_left, 0, 0) + dot(seed_up, q_right, 0, 0),
                         dot(score, seed, 0, 0)))
        for (r, u), (for_q, for_k, for_v) in zip(todo, made):
            intra_q[slot(r, u)] = for_q
            intra_k[slot(r, u)] = for_k
            intra_v[slot(r, u)] = for_v

    def arrived(r, u):
        low, up = (c_out[0, 0, u], c_out[1, 0, u]) if r == 0 else (c_in[0, r - 1, u], c_in[1, r - 1, u])
        return jnp.where(left_tall, low, up), jnp.where(left_tall, up, low)

    def finish_values(todo):
        made = [intra_v[slot(r, u)] + dot(k_ends[slot(r, u)], arrived(r, u)[1], 1, 1) for r, u in todo]
        for (r, u), block in zip(todo, made):
            d_all[tpi, rows(r, u)] = block.astype(BF16)

    def finish_rest(todo):
        kept, terms = [], []
        for r, u in todo:
            b, s = batch_of(r, u), slot(r, u)
            state, grad = arrived(r, u)
            c = cum[s]
            end = ends(c)
            grow, shrink, to_end = jnp.exp(c), jnp.exp(-c), jnp.exp(end - c)
            q, k = twice(q_v, b), twice(k_v, b)
            cross = dot(cot_v[b], state)
            dq = grow * (intra_q[s] + cross)
            dk_ = shrink * intra_k[s] + to_end * dot(val[rows(r, u)], grad)
            terms.append(q * dq - k * dk_)
            start = (jnp.sum(q * grow * cross, axis=0, keepdims=True)
                     + jnp.exp(end) * jnp.sum(state.astype(F32) * grad.astype(F32), axis=0, keepdims=True))
            kept.append((dq, dk_, start))
        for (r, u), (dq, dk_, start), sums_ in zip(todo, kept, directed(strict, terms)):
            b = batch_of(r, u)
            decay_grad = start - sums_
            o_q[b] = (dq[:, :dk] + dq[:, dk:]).astype(BF16)
            o_k[b] = (dk_[:, :dk] + dk_[:, dk:]).astype(BF16)
            o_f[b] = decay_grad[:, :dk]
            o_b[b] = decay_grad[:, dk:]

    def send_rows(u, part):
        for r in range(1, xs):
            d_copy(r, u, part).start()
        p_copy(u, part).start()

    def finish_own(u):
        finish_values([(0, u)])
        send_rows(u, 0)
        finish_rest([(0, u)])

    def first_steps(s, _):
        combine_plane(s)
        intra([(r, s) for r in range(inner)])

        @pl.when(s > 0)
        def _():
            combine_all(s - 1)
            finish_own(s - 1)
        return 0

    lax.fori_loop(0, own, first_steps, 0)
    combine_all(own - 1)
    finish_own(own - 1)

    def forward(u):
        for r in range(1, xs):
            for part in range(2):
                d_copy(r, u, part).wait_recv()
            f_copy(r, u).start()

    def features(u):
        for part in range(2):
            p_copy(u, part).wait_recv()
        for r in range(1, xs):
            f_copy(r, u).wait_recv()
        at = rows(0, u, inner)
        wide = jnp.concatenate([d_all[t, at] for t in range(tp)], 1)
        weights = jnp.concatenate([w_in[t] for t in range(tp)], 1)
        out = dot(wide, weights, 1, 1).astype(BF16)
        for r in range(inner):
            o_h[batch_of(r, u)] = out[r * length:(r + 1) * length]

    for r in range(1, tp):
        w_copy(r).wait_recv()

    def last_steps(u, _):
        others = [(r, u) for r in range(1, inner)]
        for side in range(2):
            for r in range(1, inner):
                c_copy(side, r, u).wait_recv()
        finish_values(others)
        send_rows(u, 1)
        at = rows(0, u, inner)
        w_acc[...] += dot(d_all[tpi, at], hid_v[at], 0, 0)

        @pl.when(u == own - 1)
        def _():
            for p in range(0, sp, 2):
                block = w_acc[:, p * rows_sp:(p + 2) * rows_sp].T.astype(BF16)
                g_out[p] = block[:rows_sp]
                g_out[p + 1] = block[rows_sp:]
            for r in range(1, sp):
                g_copy(r).start()

        finish_rest(others)

        @pl.when(u > 0)
        def _():
            forward(u - 1)

        @pl.when(u > 1)
        def _():
            features(u - 2)
        return 0

    lax.fori_loop(0, own, last_steps, 0)
    forward(own - 1)
    features(own - 2)
    features(own - 1)

    acc = g_out[spi].astype(F32)
    for r in range(1, sp):
        g_copy(r).wait_recv()
        acc = acc + g_in[r - 1].astype(F32)
    o_w[...] = acc

    for r in range(1, tp):
        w_copy(r).wait_send()
    for r in range(1, sp):
        e_copy(r).wait_send()
        g_copy(r).wait_send()

    def drain(u, _):
        for r in range(1, inner):
            for kind in range(2):
                a_copy(kind, r, u).wait_send()
                c_copy(kind, r, u).wait_send()
        for side in range(2):
            for r in range(1, outer):
                @pl.when(above(r) if side == 0 else below(r))
                def _():
                    b_copy(side, r, u).wait_send()
        for part in range(2):
            p_copy(u, part).wait_send()
            for r in range(1, xs):
                d_copy(r, u, part).wait_send()
        for r in range(1, xs):
            f_copy(r, u).wait_send()
        return 0

    lax.fori_loop(0, own, drain, 0)


def store_kernel(*refs):
    n = len(refs) // 2
    copies = [pltpu.make_async_copy(refs[i], refs[n + i], refs[-1].at[i]) for i in range(n)]
    for copy in copies:
        copy.start()
    for copy in copies:
        copy.wait()


def store(arrays):
    n = len(arrays)
    return pl.pallas_call(
        store_kernel,
        out_shape=tuple(jax.ShapeDtypeStruct(a.shape, a.dtype) for a in arrays),
        in_specs=[pl.BlockSpec(memory_space=pltpu.VMEM)] * n,
        out_specs=(pl.BlockSpec(memory_space=pl.ANY),) * n,
        scratch_shapes=[pltpu.SemaphoreType.DMA((n,))],
        compiler_params=pltpu.CompilerParams(has_side_effects=True, vmem_limit_bytes=1024 * 1024),
    )(*arrays)


def shards(sp, tp, hidden, value_weight, queries, key_vectors, forward_decay, backward_decay, cotangent):
    batch, length, width = hidden.shape
    heads, dk = queries.shape[1], queries.shape[3]
    dv = value_weight.shape[1]
    assert heads == 1
    inner, outer, own, xs = INNER, sp // INNER, batch // INNER, tp // CORES
    pack, rows, feat, rows_sp = 2 * dk, batch * length, width // tp, width // sp
    dims = (sp, tp, batch, length, dk, dv, width)
    vmem, dma = pltpu.VMEM, pltpu.SemaphoreType.DMA
    scratch = [
        vmem((rows, width), BF16), vmem((width, dv), BF16),
        vmem((batch, length, dk), BF16), vmem((batch, length, dk), BF16),
        vmem((batch, length, dk), F32), vmem((batch, length, dk), F32),
        vmem((batch, length, dv), BF16),
        vmem((rows, dv), BF16),
        vmem((batch, length, pack), F32),
        vmem((batch, length, pack), BF16), vmem((batch, length, pack), BF16),
        vmem((batch, length, pack), F32), vmem((batch, length, pack), F32),
        vmem((batch, length, dv), F32),
        vmem((2, inner - 1, own, dv, pack), BF16), vmem((2, inner, own, dv, pack), BF16),
        vmem((inner, own, pack), F32), vmem((sp, own, pack), F32),
        vmem((2, inner, own, dv, pack), F32),
        vmem((2, own, dv, pack), BF16), vmem((2, outer - 1, own, dv, pack), BF16),
        vmem((2, inner, own, dv, pack), BF16), vmem((2, inner - 1, own, dv, pack), BF16),
        vmem((tp, rows, dv), BF16), vmem((tp, feat, dv), BF16),
        vmem((dv, width), F32),
        vmem((sp, rows_sp, dv), BF16), vmem((sp - 1, rows_sp, dv), BF16),
        dma((6,)), dma((batch,)),
        dma((2, inner - 1, own)), dma((2, inner - 1, own)),
        dma((sp - 1,)), dma((sp - 1,)),
        dma((2, outer - 1, own)), dma((2, outer - 1, own)),
        dma((2, inner - 1, own)), dma((2, inner - 1, own)),
        dma((xs - 1, own, 2)), dma((xs - 1, own, 2)),
        dma((own, 2)), dma((own, 2)),
        dma((xs - 1, own)), dma((xs - 1, own)),
        dma((tp - 1,)), dma((tp - 1,)),
        dma((sp - 1,)), dma((sp - 1,)),
    ]
    whole = pl.BlockSpec(memory_space=vmem)
    flat = (batch, length, dk)
    args = (hidden, value_weight, queries.reshape(flat), key_vectors.reshape(flat),
            forward_decay.reshape(flat), backward_decay.reshape(flat), cotangent)
    outs = pl.pallas_call(
        functools.partial(kernel, dims),
        out_shape=(
            vmem(flat, BF16), vmem(flat, BF16), vmem(flat, F32), vmem(flat, F32),
            vmem((batch, length, feat), BF16), vmem((rows_sp, dv), F32),
        ),
        in_specs=[pl.BlockSpec(memory_space=pltpu.HBM)] * 7,
        out_specs=(whole,) * 6,
        scratch_shapes=scratch,
        compiler_params=pltpu.CompilerParams(
            collective_id=0, has_side_effects=True, vmem_limit_bytes=48 * 1024 * 1024
        ),
    )(*(pltpu.with_memory_space_constraint(a, pltpu.HBM) for a in args))
    outs = store(outs)
    return tuple(a.reshape(queries.shape) for a in outs[:4]) + tuple(outs[4:])


def solution(mesh):
    heads = P(None, "tp", "sp", None)
    return jax.shard_map(
        functools.partial(shards, mesh.shape["sp"], mesh.shape["tp"]),
        mesh=mesh,
        in_specs=(P(None, "sp", None), P(None, "tp"), heads, heads, heads, heads, P(None, "sp", "tp")),
        out_specs=(heads, heads, heads, heads, P(None, "sp", "tp"), P("sp", "tp")),
        check_vma=False,
    )
```

time: 73.1 us -> 47.5 us (0.65)
  Pallas kernels: 67.7 us -> 46.7 us
  local copies, waits for them, and re-layouts: 4.58 us -> 0 us
    pallas_call x1 -> x2, Pallas kernels: 67.7 us -> 46.7 us  [the longest x1 45.4 us: shards(): pl.pallas_call(functools.partial(kernel, dims), out_shape=(vmem(flat, BF1...]
    slice x2 -> x0, local copies, waits for them, and re-layouts: 3.25 us -> none  [the longest x1 2.37 us: shards(): decays[..., dk:]]
    unnamed x8 -> x0, local copies, waits for them, and re-layouts: 1.33 us -> none
where the time goes in v2:
time: 47.5 us; the launch traced here: 47.4 us
  Pallas kernels  46.7 us (98%)
  between operations  0.64 us (1%)
    pallas_call x1, Pallas kernels, shards(): pl.pallas_call(functools.partial(kernel, dims), out_shape=(vmem(flat, BF1...  45.4 us
    pallas_call x1, Pallas kernels, store(): pl.pallas_call(store_kernel, out_shape=tuple((jax.ShapeDtypeStruct(a.shap...  1.28 us

profile of v2, /device:TPU:1, one launch (start us, length us, event | category | flops | bytes accessed | tf_op | source)
XLA Modules:
  0.0 47.4 jit_solution(11091910143538472777)
XLA Ops:
  0.6 45.4 %shard_map.118 = (bf16[16,64,64]{2,1,0:T(8,128)(2,1)S(1)}, bf16[16,64,64]{2,1,0:T(8,128)(2,1)S(1)}, f32[16,64,64]{2,1,0:T(8,128)S(1)}, f32[16,64,64]{2,1,0:T(8,1...) custom-call(bf16[16,64,1024]{2,1,0:T(8,128)(2,1)} %hid.1, bf16[1024,128]{1,0:T(8,128)(2,1)} %wgt.1, ...), custom_call_target="tpu_custom_call" | custom-call | tf_op jit(solution)/shard_map/pallas_call | solution.py:529
  46.1 1.3 %shard_map.119 = (bf16[16,64,64]{2,1,0:T(8,128)(2,1)}, bf16[16,64,64]{2,1,0:T(8,128)(2,1)}, f32[16,64,64]{2,1,0:T(8,128)}, f32[16,64,64]{2,1,0:T(8,128)}, bf16[1...) custom-call(bf16[16,64,64]{2,1,0:T(8,128)(2,1)S(1)} %get-tuple-element.18.refs_0_, ...), custom_call_target="tpu_custom_call" | custom-call | tf_op jit(solution)/shard_map/pallas_call | solution.py:477

commit v3 on v2

v3 whole, which is shorter than its diff:
```python
import functools

import jax
import jax.numpy as jnp
from jax import lax
from jax.experimental import pallas as pl
from jax.experimental.pallas import tpu as pltpu
from jax.sharding import PartitionSpec as P

F32, BF16 = jnp.float32, jnp.bfloat16
MESH = pl.DeviceIdType.MESH
CORES = 2
INNER = 4
PLACE = (0, 2, 1, 3)
FAR_FIRST = (2, 1, 3)
OFFSETS = sorted(((dz, dy) for dz in range(4) for dy in range(4) if dz or dy),
                 key=lambda d: -sum(min(v, 4 - v) for v in d))


def dot(a, b, ca=1, cb=0):
    return lax.dot_general(a, b, (((ca,), (cb,)), ((), ())), preferred_element_type=F32)


def halves(x):
    high = x.astype(BF16)
    return jnp.concatenate([high, (x - high.astype(F32)).astype(BF16)], 0)


def kernel(dims, hid, wgt, qry, key, fdec, bdec, cot,
           o_q, o_k, o_f, o_b, o_h, o_w,
           hid_v, wgt_v, q_v, k_v, decay_v, cot_v,
           val, cum, q_hats, k_ends, intra_q, intra_k, intra_v,
           a_out, a_in, e_out, e_in, local, b_out, b_in, c_out, c_in,
           d_all, w_in, w_acc, g_out, g_in,
           i_s, h_s, a_ss, a_rs, e_ss, e_rs, b_ss, b_rs, c_ss, c_rs,
           d_ss, d_rs, f_ss, f_rs, w_ss, w_rs, g_ss, g_rs):
    sp, tp, batch, length, dk, dv, width = dims
    inner, outer, own, xs = INNER, sp // INNER, batch // INNER, tp // CORES
    pack, feat, rows_sp, group = 2 * dk, width // tp, width // sp, INNER * length
    spi, tpi = lax.axis_index("sp"), lax.axis_index("tp")
    z, y = spi // inner, lax.rem(spi, inner)
    x, core = tpi // CORES, lax.rem(tpi, CORES)

    barrier = pltpu.get_barrier_semaphore()
    for r in range(1, sp):
        pl.semaphore_signal(barrier, inc=1, device_id={"sp": lax.rem(spi + r, sp)}, device_id_type=MESH)
    for r in range(1, tp):
        pl.semaphore_signal(barrier, inc=1, device_id={"tp": lax.rem(tpi + r, tp)}, device_id_type=MESH)

    def owner(r):
        return lax.rem(y + r, inner)

    def batch_of(r, u):
        return owner(r) * own + u

    def slot(r, u):
        return u * inner + PLACE[r]

    def rows(r, u, count=1):
        return pl.ds(pl.multiple_of(slot(r, u) * length, length), count * length)

    def away(dz, dy):
        return lax.rem(z + dz, outer) * inner + lax.rem(y + dy, inner)

    bunch = 2 if own % 2 == 0 else 1

    def take(ref, sem):
        pltpu.make_async_copy(ref, ref, sem).wait()

    for i, (src, dst) in enumerate(((fdec, decay_v.at[0]), (bdec, decay_v.at[1]), (qry, q_v), (cot, cot_v),
                                    (wgt, wgt_v))):
        pltpu.make_async_copy(src, dst, i_s.at[max(i - 1, 0)]).start()
    for u in range(own):
        for r in range(inner):
            pltpu.make_async_copy(hid.at[batch_of(r, u)], hid_v.at[rows(r, u)], h_s.at[u // bunch]).start()
        if u == 0:
            pltpu.make_async_copy(key, k_v, i_s.at[4]).start()

    def remote(src, dst, ss, rs, **where):
        return pltpu.make_async_remote_copy(src_ref=src, dst_ref=dst, send_sem=ss, recv_sem=rs,
                                            device_id=where, device_id_type=MESH)

    def w_copy(r):
        to = lax.rem(tpi + r, tp)
        return remote(wgt_v.at[pl.ds(pl.multiple_of(to * feat, feat), feat), :], w_in.at[tpi],
                      w_ss.at[0], w_rs.at[0], tp=to)

    def a_copy(kind, r, u):
        return remote(a_out.at[u, kind, r - 1], a_in.at[u, kind, r], a_ss.at[0], a_rs.at[u],
                      sp=z * inner + owner(r))

    def e_copy(dz, dy):
        return remote(e_out.at[lax.rem(y + dy, inner)], e_in.at[dz * inner + dy], e_ss.at[0], e_rs.at[0],
                      sp=away(dz, dy))

    def b_copy(side, r, u):
        to = jnp.clip(z + r if side == 0 else z - r, 0, outer - 1)
        return remote(b_out.at[side, u], b_in.at[side, u, r - 1], b_ss.at[0], b_rs.at[side, u],
                      sp=to * inner + y)

    def above(r):
        return z + r < outer

    def below(r):
        return z >= r

    def c_copy(side, r, u):
        return remote(c_out.at[u, r, side], c_in.at[u, PLACE[r] - 1, side], c_ss.at[0],
                      c_rs.at[u, PLACE[r] // 2], sp=z * inner + lax.rem(y - r + inner, inner))

    mate = x * CORES + 1 - core

    def d_copies(r, u, count):
        at, half = rows(r, u, count), PLACE[r] // 2
        for k in FAR_FIRST:
            remote(d_all.at[tpi, at], d_all.at[tpi, at], d_ss.at[0], d_rs.at[k - 1, u, half],
                   tp=lax.rem(x + k, xs) * CORES + core).start()
        remote(d_all.at[tpi, at], d_all.at[tpi, at], f_ss.at[0], f_rs.at[u], tp=mate).start()

    def forward(u):
        for half in range(2):
            at = rows(half, u, 2)
            for k in (1, 3, 2):
                mine = d_all.at[lax.rem(x - k + xs, xs) * CORES + core, at]
                take(mine, d_rs.at[k - 1, u, half])
                remote(mine, mine, f_ss.at[0], f_rs.at[u], tp=mate).start()

    def g_copy(dz, dy):
        to = away(dz, dy)
        return remote(g_out.at[to], g_in.at[dz * inner + dy - 1], g_ss.at[0], g_rs.at[0], sp=to)

    row = lax.broadcasted_iota(jnp.int32, (length, length), 0)
    col = lax.broadcasted_iota(jnp.int32, (length, length), 1)
    lower, upper = row >= col, row <= col

    def matrix(first, second):
        both = jnp.concatenate([jnp.where(first, 1.0, 0.0), jnp.where(second, 1.0, 0.0)], 0)
        return jnp.concatenate([both, both], 1).astype(BF16)

    sums, strict = matrix(lower, upper), matrix(row > col, row < col)
    left = lax.broadcasted_iota(jnp.int32, (length, pack), 1) < dk
    left_tall = lax.broadcasted_iota(jnp.int32, (dv, pack), 1) < dk

    def directed(tri, blocks):
        made = []
        for i in range(0, len(blocks), 2):
            pair = blocks[i:i + 2]
            out = dot(tri, halves(jnp.concatenate(pair, 1) if len(pair) > 1 else pair[0]))
            for n in range(len(pair)):
                part = out[:, n * pack:(n + 1) * pack]
                made.append(jnp.where(left, part[:length], part[length:]))
        return made

    def twice(ref, b):
        v = ref[b].astype(F32)
        return jnp.concatenate([v, v], 1)

    def ends(c):
        return jnp.where(left[:1], c[length - 1:length], c[0:1])

    for side in range(2):
        for r in range(1, outer):
            @pl.when(jnp.logical_not(below(r) if side == 0 else above(r)))
            def _():
                b_in[side, :, r - 1] = jnp.zeros((own, dv, pack), BF16)

    def decays(todo):
        blocks = [jnp.concatenate([decay_v[0, batch_of(r, u)], decay_v[1, batch_of(r, u)]], 1) for r, u in todo]
        made = directed(sums, blocks)
        for (r, u), c in zip(todo, made):
            cum[slot(r, u)] = c
        for (r, u), c in zip(todo, made):
            e_out[owner(r), pl.ds(u, 1), :] = ends(c)

    take(decay_v, i_s.at[0])
    decays([(r, u) for u in range(own) for r in range(inner)])

    def grads(todo):
        hats = [(twice(q_v, batch_of(r, u)) * jnp.exp(cum[slot(r, u)])).astype(BF16) for r, u in todo]
        made = [dot(cot_v[batch_of(r, u)], hat, 0, 0).astype(BF16) for (r, u), hat in zip(todo, hats)]
        return hats, made

    def states(todo):
        keys = []
        for r, u in todo:
            c = cum[slot(r, u)]
            keys.append((twice(k_v, batch_of(r, u)) * jnp.exp(ends(c) - c)).astype(BF16))
        made = [dot(val[rows(r, u)], k_end, 0, 0).astype(BF16) for (r, u), k_end in zip(todo, keys)]
        return keys, made

    def place(kind, r, u, value):
        if r == 0:
            a_in[u, kind, 0] = value
        else:
            a_out[u, kind, r - 1] = value

    def emit(kind, todo):
        kept, made = (grads if kind == 0 else states)(todo)
        keep = q_hats if kind == 0 else k_ends
        for (r, u), value, block in zip(todo, kept, made):
            keep[slot(r, u)] = value
            place(kind, r, u, block)

    def values(u):
        at = rows(0, u, inner)
        val[at] = dot(hid_v[at], wgt_v[...]).astype(BF16)

    take(q_v, i_s.at[1])
    take(cot_v, i_s.at[2])

    for first in range(0, own, bunch):
        todo = [(r, first + n) for n in range(bunch) for r in FAR_FIRST]
        emit(0, todo)
        if first == 0:
            pl.semaphore_wait(barrier, sp + tp - 2)
            for offset in OFFSETS:
                e_copy(*offset).start()
        for r, u in todo:
            a_copy(0, r, u).start()
        if first == 0:
            take(wgt_v, i_s.at[3])
            for r in range(1, tp):
                w_copy(r).start()
            w_in[tpi] = wgt_v[pl.ds(pl.multiple_of(tpi * feat, feat), feat), :]
            e_in[0] = e_out[y]
            take(k_v, i_s.at[4])
        take(hid_v.at[rows(0, first, bunch * inner)], h_s.at[first // bunch])
        for n in range(bunch):
            values(first + n)
        emit(1, todo)
        for r, u in todo:
            a_copy(1, r, u).start()

    mine = [(0, u) for u in range(own)]
    emit(0, mine)
    emit(1, mine)
    w_acc[...] = jnp.zeros((dv, width), F32)

    def ending(plane, person, u):
        source = lax.rem(z - plane + outer, outer) * inner + lax.rem(y - person + inner, inner)
        return e_in[source, pl.ds(u, 1), :]

    people = (tuple(range(inner)), tuple(range(inner - 1, -1, -1)))

    def offset(person):
        return lax.rem(y - person + inner, inner)

    def combine_plane(u):
        take(a_in.at[u, :, pl.ds(1, inner - 1)], a_rs.at[u])
        for side in range(2):
            running = jnp.zeros((dv, pack), F32)
            for n, person in enumerate(people[side]):
                grad, state = a_in[u, 0, offset(person)], a_in[u, 1, offset(person)]
                block = jnp.where(left_tall, state, grad) if side == 0 else jnp.where(left_tall, grad, state)
                if n == 0:
                    running = block.astype(F32)
                else:
                    local[side, person, u] = running
                    running = jnp.exp(ending(z, person, u)) * running + block.astype(F32)
            b_out[side, u] = running.astype(BF16)
        for side in range(2):
            for r in range(1, outer):
                @pl.when(above(r) if side == 0 else below(r))
                def _():
                    b_copy(side, r, u).start()

    def combine_all(u):
        for side in range(2):
            for n in range(1, outer):
                @pl.when((z if side == 0 else outer - 1 - z) == n)
                def _():
                    take(b_in.at[side, u, pl.ds(0, n)], b_rs.at[side, u])
        for side in range(2):
            carried = b_in[side, u, 0].astype(F32)
            passed = jnp.zeros((1, pack), F32)
            for r in range(2, outer):
                plane = lax.rem(z - r + 1 + outer, outer) if side == 0 else lax.rem(z + r - 1, outer)
                for person in range(inner):
                    passed = passed + ending(plane, person, u)
                carried = carried + jnp.exp(passed) * b_in[side, u, r - 1].astype(F32)
            passed = jnp.zeros((1, pack), F32)
            for n, person in enumerate(people[side]):
                if n == 0:
                    c_out[u, offset(person), side] = carried.astype(BF16)
                else:
                    out = jnp.exp(passed) * carried + local[side, person, u]
                    c_out[u, offset(person), side] = out.astype(BF16)
                passed = passed + ending(z, person, u)
        for r in FAR_FIRST:
            for side in range(2):
                c_copy(side, r, u).start()

    def intra(todo):
        made = []
        for r, u in todo:
            b, s = batch_of(r, u), slot(r, u)
            q_hat = q_hats[s]
            k_hat = (twice(k_v, b) * jnp.exp(-cum[s])).astype(BF16)
            v, seed = val[rows(r, u)], cot_v[b]
            seed_scores = dot(seed, v, 1, 1)
            zero = jnp.zeros_like(q_hat)
            q_left, q_right = jnp.where(left, q_hat, zero), jnp.where(left, zero, q_hat)
            k_left, k_right = jnp.where(left, k_hat, zero), jnp.where(left, zero, k_hat)
            score = (jnp.where(lower, dot(q_left, k_hat, 1, 1), 0.0)
                     + jnp.where(upper, dot(q_right, k_hat, 1, 1), 0.0)).astype(BF16)
            seed_low = jnp.where(lower, seed_scores, 0.0).astype(BF16)
            seed_up = jnp.where(upper, seed_scores, 0.0).astype(BF16)
            made.append((dot(seed_low, k_left) + dot(seed_up, k_right),
                         dot(seed_low, q_left, 0, 0) + dot(seed_up, q_right, 0, 0),
                         dot(score, seed, 0, 0)))
        for (r, u), (for_q, for_k, for_v) in zip(todo, made):
            intra_q[slot(r, u)] = for_q
            intra_k[slot(r, u)] = for_k
            intra_v[slot(r, u)] = for_v

    def arrived(r, u):
        low, up = (c_out[u, 0, 0], c_out[u, 0, 1]) if r == 0 else (c_in[u, PLACE[r] - 1, 0], c_in[u, PLACE[r] - 1, 1])
        return jnp.where(left_tall, low, up), jnp.where(left_tall, up, low)

    def finish_values(todo):
        made = [intra_v[slot(r, u)] + dot(k_ends[slot(r, u)], arrived(r, u)[1], 1, 1) for r, u in todo]
        for (r, u), block in zip(todo, made):
            d_all[tpi, rows(r, u)] = block.astype(BF16)

    def finish_rest(todo):
        kept, terms = [], []
        for r, u in todo:
            b, s = batch_of(r, u), slot(r, u)
            state, grad = arrived(r, u)
            c = cum[s]
            end = ends(c)
            grow, shrink, to_end = jnp.exp(c), jnp.exp(-c), jnp.exp(end - c)
            q, k = twice(q_v, b), twice(k_v, b)
            cross = dot(cot_v[b], state)
            dq = grow * (intra_q[s] + cross)
            dk_ = shrink * intra_k[s] + to_end * dot(val[rows(r, u)], grad)
            terms.append(q * dq - k * dk_)
            start = (jnp.sum(q * grow * cross, axis=0, keepdims=True)
                     + jnp.exp(end) * jnp.sum(state.astype(F32) * grad.astype(F32), axis=0, keepdims=True))
            kept.append((dq, dk_, start))
        for (r, u), (dq, dk_, start), sums_ in zip(todo, kept, directed(strict, terms)):
            b = batch_of(r, u)
            decay_grad = start - sums_
            o_q[b] = (dq[:, :dk] + dq[:, dk:]).astype(BF16)
            o_k[b] = (dk_[:, :dk] + dk_[:, dk:]).astype(BF16)
            o_f[b] = decay_grad[:, :dk]
            o_b[b] = decay_grad[:, dk:]

    def finish_own(u):
        finish_values([(0, u)])
        d_copies(0, u, 1)
        finish_rest([(0, u)])

    def features(u):
        take(d_all.at[pl.ds(0, xs), rows(0, u, inner)], f_rs.at[u])
        at = rows(0, u, inner)
        wide = jnp.concatenate([d_all[t, at] for t in range(tp)], 1)
        weights = jnp.concatenate([w_in[t] for t in range(tp)], 1)
        out = dot(wide, weights, 1, 1).astype(BF16)
        for r in range(inner):
            o_h[batch_of(r, u)] = out[PLACE[r] * length:(PLACE[r] + 1) * length]

    def finish_others(todo, u):
        first = PLACE[todo[0]] - 1
        take(c_in.at[u, pl.ds(first, len(todo))], c_rs.at[u, (first + 1) // 2])
        todo = [(r, u) for r in todo]
        finish_values(todo)
        d_copies(*todo[0], len(todo))

    def weight_terms(r, u):
        at = rows(r, u, 2)
        return dot(d_all[tpi, at], hid_v[at], 0, 0)

    def others(u):
        finish_others([2], u)
        finish_others([1, 3], u)
        at = rows(0, u, inner)
        w_acc[...] += dot(d_all[tpi, at], hid_v[at], 0, 0)
        finish_rest([(r, u) for r in range(1, inner)])

    def combine_and_finish(u):
        combine_all(u)
        finish_own(u)

    def loop(first, last, step):
        lax.fori_loop(first, last, lambda u, _: step(u) or 0, 0)

    def intra_all(u):
        intra([(r, u) for r in range(inner)])

    def late_steps(u):
        combine_and_finish(u)
        others(u - own // 2)

    loop(0, own - 1, intra_all)
    take(e_in.at[pl.ds(1, sp - 1)], e_rs.at[0])
    combine_plane(0)
    intra_all(own - 1)
    loop(1, own // 2, combine_plane)
    loop(0, own // 2, combine_and_finish)
    loop(own // 2, own, combine_plane)
    loop(own // 2, own, late_steps)
    loop(own - own // 2, own - 1, others)
    take(w_in.at[pl.ds(0, tp - 1)], w_rs.at[0])
    loop(0, own - 2, forward)
    loop(0, own - 3, features)

    end = own - 1
    finish_others([2], end)
    w_acc[...] += weight_terms(0, end)
    finish_others([1, 3], end)
    full = w_acc[...] + weight_terms(1, end)
    for p in range(0, sp, 2):
        block = full[:, p * rows_sp:(p + 2) * rows_sp].T.astype(BF16)
        g_out[p] = block[:rows_sp]
        g_out[p + 1] = block[rows_sp:]
    for offset in OFFSETS:
        g_copy(*offset).start()
    finish_rest([(r, end) for r in range(1, inner)])
    forward(end - 1)
    loop(own - 3, own - 2, features)
    forward(end)
    loop(own - 2, own, features)

    take(g_in, g_rs.at[0])
    acc = g_out[spi].astype(F32)
    for r in range(sp - 1):
        acc = acc + g_in[r].astype(F32)
    o_w[...] = acc

    take(w_in.at[pl.ds(0, tp - 1)], w_ss.at[0])
    take(e_in.at[pl.ds(1, sp - 1)], e_ss.at[0])
    take(a_out, a_ss.at[0])
    take(b_in.at[0], b_ss.at[0])
    take(c_in, c_ss.at[0])
    take(d_all.at[pl.ds(0, xs - 1)], d_ss.at[0])
    take(d_all.at[pl.ds(0, xs)], f_ss.at[0])
    take(g_in, g_ss.at[0])


def store_kernel(*refs):
    n = len(refs) // 2
    copies = [pltpu.make_async_copy(refs[i], refs[n + i], refs[-1].at[i]) for i in range(n)]
    for copy in copies:
        copy.start()
    for copy in copies:
        copy.wait()


def store(arrays):
    n = len(arrays)
    return pl.pallas_call(
        store_kernel,
        out_shape=tuple(jax.ShapeDtypeStruct(a.shape, a.dtype) for a in arrays),
        in_specs=[pl.BlockSpec(memory_space=pltpu.VMEM)] * n,
        out_specs=(pl.BlockSpec(memory_space=pl.ANY),) * n,
        scratch_shapes=[pltpu.SemaphoreType.DMA((n,))],
        compiler_params=pltpu.CompilerParams(has_side_effects=True, vmem_limit_bytes=1024 * 1024),
    )(*arrays)


def shards(sp, tp, hidden, value_weight, queries, key_vectors, forward_decay, backward_decay, cotangent):
    batch, length, width = hidden.shape
    heads, dk = queries.shape[1], queries.shape[3]
    dv = value_weight.shape[1]
    assert heads == 1
    inner, outer, own, xs = INNER, sp // INNER, batch // INNER, tp // CORES
    pack, rows, feat, rows_sp = 2 * dk, batch * length, width // tp, width // sp
    dims = (sp, tp, batch, length, dk, dv, width)
    vmem, dma = pltpu.VMEM, pltpu.SemaphoreType.DMA
    scratch = [
        vmem((rows, width), BF16), vmem((width, dv), BF16),
        vmem((batch, length, dk), BF16), vmem((batch, length, dk), BF16),
        vmem((2, batch, length, dk), F32), vmem((batch, length, dv), BF16),
        vmem((rows, dv), BF16),
        vmem((batch, length, pack), F32),
        vmem((batch, length, pack), BF16), vmem((batch, length, pack), BF16),
        vmem((batch, length, pack), F32), vmem((batch, length, pack), F32),
        vmem((batch, length, dv), F32),
        vmem((own, 2, inner - 1, dv, pack), BF16), vmem((own, 2, inner, dv, pack), BF16),
        vmem((inner, own, pack), F32), vmem((sp, own, pack), F32),
        vmem((2, inner, own, dv, pack), F32),
        vmem((2, own, dv, pack), BF16), vmem((2, own, outer - 1, dv, pack), BF16),
        vmem((own, inner, 2, dv, pack), BF16), vmem((own, inner - 1, 2, dv, pack), BF16),
        vmem((tp, rows, dv), BF16), vmem((tp, feat, dv), BF16),
        vmem((dv, width), F32),
        vmem((sp, rows_sp, dv), BF16), vmem((sp - 1, rows_sp, dv), BF16),
        dma((5,)), dma((2,)),
        dma((1,)), dma((own,)),
        dma((1,)), dma((1,)),
        dma((1,)), dma((2, own)),
        dma((1,)), dma((own, 2)),
        dma((1,)), dma((xs - 1, own, 2)),
        dma((1,)), dma((own,)),
        dma((1,)), dma((1,)),
        dma((1,)), dma((1,)),
    ]
    whole = pl.BlockSpec(memory_space=vmem)
    flat = (batch, length, dk)
    args = (hidden, value_weight, queries.reshape(flat), key_vectors.reshape(flat),
            forward_decay.reshape(flat), backward_decay.reshape(flat), cotangent)
    outs = pl.pallas_call(
        functools.partial(kernel, dims),
        out_shape=(
            vmem(flat, BF16), vmem(flat, BF16), vmem(flat, F32), vmem(flat, F32),
            vmem((batch, length, feat), BF16), vmem((rows_sp, dv), F32),
        ),
        in_specs=[pl.BlockSpec(memory_space=pltpu.HBM)] * 7,
        out_specs=(whole,) * 6,
        scratch_shapes=scratch,
        compiler_params=pltpu.CompilerParams(
            collective_id=0, has_side_effects=True, vmem_limit_bytes=48 * 1024 * 1024
        ),
    )(*(pltpu.with_memory_space_constraint(a, pltpu.HBM) for a in args))
    outs = store(outs)
    return tuple(a.reshape(queries.shape) for a in outs[:4]) + tuple(outs[4:])


def solution(mesh):
    heads = P(None, "tp", "sp", None)
    return jax.shard_map(
        functools.partial(shards, mesh.shape["sp"], mesh.shape["tp"]),
        mesh=mesh,
        in_specs=(P(None, "sp", None), P(None, "tp"), heads, heads, heads, heads, P(None, "sp", "tp")),
        out_specs=(heads, heads, heads, heads, P(None, "sp", "tp"), P("sp", "tp")),
        check_vma=False,
    )
```

time: 47.5 us -> 43.1 us (0.907)
  Pallas kernels: 46.7 us -> 42.3 us
    pallas_call x1, Pallas kernels: 45.4 us -> 41.1 us  [shards(): pl.pallas_call(functools.partial(kernel, dims), out_shape=(vmem(flat, BF1...]
where the time goes in v3:
time: 43.1 us; the launch traced here: 43 us
  Pallas kernels  42.3 us (98%)
  between operations  0.64 us (1%)
    pallas_call x1, Pallas kernels, shards(): pl.pallas_call(functools.partial(kernel, dims), out_shape=(vmem(flat, BF1...  41.1 us
    pallas_call x1, Pallas kernels, store(): pl.pallas_call(store_kernel, out_shape=tuple((jax.ShapeDtypeStruct(a.shap...  1.28 us

profile of v3, /device:TPU:1, one launch (start us, length us, event | category | flops | bytes accessed | tf_op | source)
XLA Modules:
  0.0 43.0 jit_solution(2522748224031034985)
XLA Ops:
  0.6 41.1 %shard_map.118 = (bf16[16,64,64]{2,1,0:T(8,128)(2,1)S(1)}, bf16[16,64,64]{2,1,0:T(8,128)(2,1)S(1)}, f32[16,64,64]{2,1,0:T(8,128)S(1)}, f32[16,64,64]{2,1,0:T(8,1...) custom-call(bf16[16,64,1024]{2,1,0:T(8,128)(2,1)} %hid.1, bf16[1024,128]{1,0:T(8,128)(2,1)} %wgt.1, ...), custom_call_target="tpu_custom_call" | custom-call | tf_op jit(solution)/shard_map/pallas_call | solution.py:502
  41.7 1.3 %shard_map.119 = (bf16[16,64,64]{2,1,0:T(8,128)(2,1)}, bf16[16,64,64]{2,1,0:T(8,128)(2,1)}, f32[16,64,64]{2,1,0:T(8,128)}, f32[16,64,64]{2,1,0:T(8,128)}, bf16[1...) custom-call(bf16[16,64,64]{2,1,0:T(8,128)(2,1)S(1)} %get-tuple-element.18.refs_0_, ...), custom_call_target="tpu_custom_call" | custom-call | tf_op jit(solution)/shard_map/pallas_call | solution.py:452

commit v4 on v3

--- a/solution.py
+++ b/solution.py
@@ -42,39 +42,53 @@
     x, core = tpi // CORES, lax.rem(tpi, CORES)
 
     barrier = pltpu.get_barrier_semaphore()
+    def owner(r):
+        return lax.rem(y + r, inner)
+
+    def batch_of(r, u):
+        return owner(r) * own + u
+
+    def slot(r, u):
+        return u * inner + PLACE[r]
+
+    def rows(r, u, count=1):
+        return pl.ds(pl.multiple_of(slot(r, u) * length, length), count * length)
+
+    def away(dz, dy):
+        return lax.rem(z + dz, outer) * inner + lax.rem(y + dy, inner)
+
+    def take(ref, sem):
+        pltpu.make_async_copy(ref, ref, sem).wait()
+
+    def load(first, count):
+        at, n = pl.ds(first, count), min(first, 1)
+        for i in range(2):
+            pltpu.make_async_copy((fdec, bdec)[i].at[:, at], decay_v.at[i, :, at], i_s.at[n]).start()
+        pltpu.make_async_copy(qry.at[:, at], q_v.at[:, at], i_s.at[2 + n]).start()
+        pltpu.make_async_copy(cot.at[:, at], cot_v.at[:, at], i_s.at[4 + n]).start()
+
+    def loaded(first, count):
+        at, n = pl.ds(first, count), min(first, 1)
+        take(decay_v.at[:, :, at], i_s.at[n])
+        take(q_v.at[:, at], i_s.at[2 + n])
+        take(cot_v.at[:, at], i_s.at[4 + n])
+
+    def load_hidden(u):
+        for r in range(inner):
+            pltpu.make_async_copy(hid.at[owner(r), u], hid_v.at[rows(r, u)], h_s.at[u]).start()
+
+    load(0, 1)
     for r in range(1, sp):
         pl.semaphore_signal(barrier, inc=1, device_id={"sp": lax.rem(spi + r, sp)}, device_id_type=MESH)
     for r in range(1, tp):
         pl.semaphore_signal(barrier, inc=1, device_id={"tp": lax.rem(tpi + r, tp)}, device_id_type=MESH)
 
-    def owner(r):
-        return lax.rem(y + r, inner)
-
-    def batch_of(r, u):
-        return owner(r) * own + u
-
-    def slot(r, u):
-        return u * inner + PLACE[r]
-
-    def rows(r, u, count=1):
-        return pl.ds(pl.multiple_of(slot(r, u) * length, length), count * length)
-
-    def away(dz, dy):
-        return lax.rem(z + dz, outer) * inner + lax.rem(y + dy, inner)
-
-    bunch = 2 if own % 2 == 0 else 1
-
-    def take(ref, sem):
-        pltpu.make_async_copy(ref, ref, sem).wait()
-
-    for i, (src, dst) in enumerate(((fdec, decay_v.at[0]), (bdec, decay_v.at[1]), (qry, q_v), (cot, cot_v),
-                                    (wgt, wgt_v))):
-        pltpu.make_async_copy(src, dst, i_s.at[max(i - 1, 0)]).start()
-    for u in range(own):
-        for r in range(inner):
-            pltpu.make_async_copy(hid.at[batch_of(r, u)], hid_v.at[rows(r, u)], h_s.at[u // bunch]).start()
-        if u == 0:
-            pltpu.make_async_copy(key, k_v, i_s.at[4]).start()
+    pltpu.make_async_copy(wgt, wgt_v, i_s.at[6]).start()
+    load_hidden(0)
+    pltpu.make_async_copy(key, k_v, i_s.at[7]).start()
+    load(1, own - 1)
+    for u in range(1, own):
+        load_hidden(u)
 
     def remote(src, dst, ss, rs, **where):
         return pltpu.make_async_remote_copy(src_ref=src, dst_ref=dst, send_sem=ss, recv_sem=rs,
@@ -95,7 +109,7 @@
 
     def b_copy(side, r, u):
         to = jnp.clip(z + r if side == 0 else z - r, 0, outer - 1)
-        return remote(b_out.at[side, u], b_in.at[side, u, r - 1], b_ss.at[0], b_rs.at[side, u],
+        return remote(b_out.at[side, u], b_in.at[side, u, r - 1], b_ss.at[0], b_rs.at[u],
                       sp=to * inner + y)
 
     def above(r):
@@ -113,16 +127,16 @@
     def d_copies(r, u, count):
         at, half = rows(r, u, count), PLACE[r] // 2
         for k in FAR_FIRST:
-            remote(d_all.at[tpi, at], d_all.at[tpi, at], d_ss.at[0], d_rs.at[k - 1, u, half],
+            remote(d_all.at[tpi, at], d_all.at[tpi, at], d_ss.at[0], d_rs.at[u, half],
                    tp=lax.rem(x + k, xs) * CORES + core).start()
         remote(d_all.at[tpi, at], d_all.at[tpi, at], f_ss.at[0], f_rs.at[u], tp=mate).start()
 
     def forward(u):
         for half in range(2):
             at = rows(half, u, 2)
-            for k in (1, 3, 2):
+            take(d_all.at[pl.ds(0, xs - 1), at], d_rs.at[u, half])
+            for k in range(1, xs):
                 mine = d_all.at[lax.rem(x - k + xs, xs) * CORES + core, at]
-                take(mine, d_rs.at[k - 1, u, half])
                 remote(mine, mine, f_ss.at[0], f_rs.at[u], tp=mate).start()
 
     def g_copy(dz, dy):
@@ -151,8 +165,8 @@
                 made.append(jnp.where(left, part[:length], part[length:]))
         return made
 
-    def twice(ref, b):
-        v = ref[b].astype(F32)
+    def twice(ref, r, u):
+        v = ref[owner(r), u].astype(F32)
         return jnp.concatenate([v, v], 1)
 
     def ends(c):
@@ -165,26 +179,23 @@
                 b_in[side, :, r - 1] = jnp.zeros((own, dv, pack), BF16)
 
     def decays(todo):
-        blocks = [jnp.concatenate([decay_v[0, batch_of(r, u)], decay_v[1, batch_of(r, u)]], 1) for r, u in todo]
+        blocks = [jnp.concatenate([decay_v[0, owner(r), u], decay_v[1, owner(r), u]], 1) for r, u in todo]
         made = directed(sums, blocks)
         for (r, u), c in zip(todo, made):
             cum[slot(r, u)] = c
         for (r, u), c in zip(todo, made):
             e_out[owner(r), pl.ds(u, 1), :] = ends(c)
 
-    take(decay_v, i_s.at[0])
-    decays([(r, u) for u in range(own) for r in range(inner)])
-
     def grads(todo):
-        hats = [(twice(q_v, batch_of(r, u)) * jnp.exp(cum[slot(r, u)])).astype(BF16) for r, u in todo]
-        made = [dot(cot_v[batch_of(r, u)], hat, 0, 0).astype(BF16) for (r, u), hat in zip(todo, hats)]
+        hats = [(twice(q_v, r, u) * jnp.exp(cum[slot(r, u)])).astype(BF16) for r, u in todo]
+        made = [dot(cot_v[owner(r), u], hat, 0, 0).astype(BF16) for (r, u), hat in zip(todo, hats)]
         return hats, made
 
     def states(todo):
         keys = []
         for r, u in todo:
             c = cum[slot(r, u)]
-            keys.append((twice(k_v, batch_of(r, u)) * jnp.exp(ends(c) - c)).astype(BF16))
+            keys.append((twice(k_v, r, u) * jnp.exp(ends(c) - c)).astype(BF16))
         made = [dot(val[rows(r, u)], k_end, 0, 0).astype(BF16) for (r, u), k_end in zip(todo, keys)]
         return keys, made
 
@@ -205,32 +216,34 @@
         at = rows(0, u, inner)
         val[at] = dot(hid_v[at], wgt_v[...]).astype(BF16)
 
-    take(q_v, i_s.at[1])
-    take(cot_v, i_s.at[2])
-
-    for first in range(0, own, bunch):
-        todo = [(r, first + n) for n in range(bunch) for r in FAR_FIRST]
+    everyone = tuple(range(inner))
+    for u in range(own):
+        todo = [(r, u) for r in FAR_FIRST]
+        if u == 0:
+            loaded(0, 1)
+            decays([(r, u) for r in everyone])
         emit(0, todo)
-        if first == 0:
+        if u == 0:
             pl.semaphore_wait(barrier, sp + tp - 2)
+        for r, u in todo:
+            a_copy(0, r, u).start()
+        if u == 0:
+            loaded(1, own - 1)
+            decays([(r, n) for n in range(1, own) for r in everyone])
             for offset in OFFSETS:
                 e_copy(*offset).start()
-        for r, u in todo:
-            a_copy(0, r, u).start()
-        if first == 0:
-            take(wgt_v, i_s.at[3])
-            for r in range(1, tp):
-                w_copy(r).start()
-            w_in[tpi] = wgt_v[pl.ds(pl.multiple_of(tpi * feat, feat), feat), :]
-            e_in[0] = e_out[y]
-            take(k_v, i_s.at[4])
-        take(hid_v.at[rows(0, first, bunch * inner)], h_s.at[first // bunch])
-        for n in range(bunch):
-            values(first + n)
+            take(wgt_v, i_s.at[6])
+            take(k_v, i_s.at[7])
+        take(hid_v.at[rows(0, u, inner)], h_s.at[u])
+        values(u)
         emit(1, todo)
         for r, u in todo:
             a_copy(1, r, u).start()
 
+    for r in range(1, tp):
+        w_copy(r).start()
+    w_in[tpi] = wgt_v[pl.ds(pl.multiple_of(tpi * feat, feat), feat), :]
+    e_in[0] = e_out[y]
     mine = [(0, u) for u in range(own)]
     emit(0, mine)
     emit(1, mine)
@@ -265,11 +278,7 @@
                     b_copy(side, r, u).start()
 
     def combine_all(u):
-        for side in range(2):
-            for n in range(1, outer):
-                @pl.when((z if side == 0 else outer - 1 - z) == n)
-                def _():
-                    take(b_in.at[side, u, pl.ds(0, n)], b_rs.at[side, u])
+        take(b_in.at[0, u], b_rs.at[u])
         for side in range(2):
             carried = b_in[side, u, 0].astype(F32)
             passed = jnp.zeros((1, pack), F32)
@@ -293,10 +302,10 @@
     def intra(todo):
         made = []
         for r, u in todo:
-            b, s = batch_of(r, u), slot(r, u)
+            s = slot(r, u)
             q_hat = q_hats[s]
-            k_hat = (twice(k_v, b) * jnp.exp(-cum[s])).astype(BF16)
-            v, seed = val[rows(r, u)], cot_v[b]
+            k_hat = (twice(k_v, r, u) * jnp.exp(-cum[s])).astype(BF16)
+            v, seed = val[rows(r, u)], cot_v[owner(r), u]
             seed_scores = dot(seed, v, 1, 1)
             zero = jnp.zeros_like(q_hat)
             q_left, q_right = jnp.where(left, q_hat, zero), jnp.where(left, zero, q_hat)
@@ -325,13 +334,13 @@
     def finish_rest(todo):
         kept, terms = [], []
         for r, u in todo:
-            b, s = batch_of(r, u), slot(r, u)
+            s = slot(r, u)
             state, grad = arrived(r, u)
             c = cum[s]
             end = ends(c)
             grow, shrink, to_end = jnp.exp(c), jnp.exp(-c), jnp.exp(end - c)
-            q, k = twice(q_v, b), twice(k_v, b)
-            cross = dot(cot_v[b], state)
+            q, k = twice(q_v, r, u), twice(k_v, r, u)
+            cross = dot(cot_v[owner(r), u], state)
             dq = grow * (intra_q[s] + cross)
             dk_ = shrink * intra_k[s] + to_end * dot(val[rows(r, u)], grad)
             terms.append(q * dq - k * dk_)
@@ -378,34 +387,32 @@
         w_acc[...] += dot(d_all[tpi, at], hid_v[at], 0, 0)
         finish_rest([(r, u) for r in range(1, inner)])
 
-    def combine_and_finish(u):
+    def loop(first, last, step):
+        lax.fori_loop(first, last, lambda u, _: step(u) or 0, 0)
+
+    def intra_all(u):
+        intra([(r, u) for r in range(inner)])
+
+    def middle_steps(u):
         combine_all(u)
         finish_own(u)
-
-    def loop(first, last, step):
-        lax.fori_loop(first, last, lambda u, _: step(u) or 0, 0)
-
-    def intra_all(u):
-        intra([(r, u) for r in range(inner)])
+        combine_plane(u + half_own)
 
     def late_steps(u):
-        combine_and_finish(u)
-        others(u - own // 2)
-
-    loop(0, own - 1, intra_all)
+        combine_all(u)
+        finish_own(u)
+        others(u - half_own)
+
+    half_own, end = own // 2, own - 1
+    loop(0, half_own, intra_all)
     take(e_in.at[pl.ds(1, sp - 1)], e_rs.at[0])
     combine_plane(0)
-    intra_all(own - 1)
-    loop(1, own // 2, combine_plane)
-    loop(0, own // 2, combine_and_finish)
-    loop(own // 2, own, combine_plane)
-    loop(own // 2, own, late_steps)
-    loop(own - own // 2, own - 1, others)
-    take(w_in.at[pl.ds(0, tp - 1)], w_rs.at[0])
-    loop(0, own - 2, forward)
-    loop(0, own - 3, features)
-
-    end = own - 1
+    loop(half_own, own, intra_all)
+    loop(1, half_own, combine_plane)
+    loop(0, half_own, middle_steps)
+    loop(half_own, own, late_steps)
+    loop(half_own, end, others)
+
     finish_others([2], end)
     w_acc[...] += weight_terms(0, end)
     finish_others([1, 3], end)
@@ -417,10 +424,11 @@
     for offset in OFFSETS:
         g_copy(*offset).start()
     finish_rest([(r, end) for r in range(1, inner)])
-    forward(end - 1)
-    loop(own - 3, own - 2, features)
+    loop(0, end, forward)
+    take(w_in.at[pl.ds(0, tp - 1)], w_rs.at[0])
+    loop(0, half_own, features)
     forward(end)
-    loop(own - 2, own, features)
+    loop(half_own, own, features)
 
     take(g_in, g_rs.at[0])
     acc = g_out[spi].astype(F32)
@@ -470,8 +478,8 @@
     vmem, dma = pltpu.VMEM, pltpu.SemaphoreType.DMA
     scratch = [
         vmem((rows, width), BF16), vmem((width, dv), BF16),
-        vmem((batch, length, dk), BF16), vmem((batch, length, dk), BF16),
-        vmem((2, batch, length, dk), F32), vmem((batch, length, dv), BF16),
+        vmem((inner, own, length, dk), BF16), vmem((inner, own, length, dk), BF16),
+        vmem((2, inner, own, length, dk), F32), vmem((inner, own, length, dv), BF16),
         vmem((rows, dv), BF16),
         vmem((batch, length, pack), F32),
         vmem((batch, length, pack), BF16), vmem((batch, length, pack), BF16),
@@ -485,20 +493,21 @@
         vmem((tp, rows, dv), BF16), vmem((tp, feat, dv), BF16),
         vmem((dv, width), F32),
         vmem((sp, rows_sp, dv), BF16), vmem((sp - 1, rows_sp, dv), BF16),
-        dma((5,)), dma((2,)),
+        dma((8,)), dma((own,)),
         dma((1,)), dma((own,)),
         dma((1,)), dma((1,)),
-        dma((1,)), dma((2, own)),
+        dma((1,)), dma((own,)),
         dma((1,)), dma((own, 2)),
-        dma((1,)), dma((xs - 1, own, 2)),
+        dma((1,)), dma((own, 2)),
         dma((1,)), dma((own,)),
         dma((1,)), dma((1,)),
         dma((1,)), dma((1,)),
     ]
     whole = pl.BlockSpec(memory_space=vmem)
-    flat = (batch, length, dk)
-    args = (hidden, value_weight, queries.reshape(flat), key_vectors.reshape(flat),
-            forward_decay.reshape(flat), backward_decay.reshape(flat), cotangent)
+    flat, split = (batch, length, dk), (inner, own, length, dk)
+    args = (hidden.reshape(inner, own, length, width), value_weight, queries.reshape(split),
+            key_vectors.reshape(split), forward_decay.reshape(split), backward_decay.reshape(split),
+            cotangent.reshape(inner, own, length, dv))
     outs = pl.pallas_call(
         functools.partial(kernel, dims),
         out_shape=(

time: 43.1 us -> 41.6 us (0.965)
  Pallas kernels: 42.3 us -> 40.8 us
    pallas_call x1, Pallas kernels: 41.1 us -> 39.5 us  [shards(): pl.pallas_call(functools.partial(kernel, dims), out_shape=(vmem(flat, BF1...]
where the time goes in v4:
time: 41.6 us; the launch traced here: 41.4 us
  Pallas kernels  40.8 us (98%)
  between operations  0.64 us (2%)
    pallas_call x1, Pallas kernels, shards(): pl.pallas_call(functools.partial(kernel, dims), out_shape=(vmem(flat, BF1...  39.5 us
    pallas_call x1, Pallas kernels, store(): pl.pallas_call(store_kernel, out_shape=tuple((jax.ShapeDtypeStruct(a.shap...  1.28 us

profile of v4, /device:TPU:1, one launch (start us, length us, event | category | flops | bytes accessed | tf_op | source)
XLA Modules:
  0.0 41.4 jit_solution(16034534000733701746)
XLA Ops:
  0.6 39.5 %shard_map.118 = (bf16[16,64,64]{2,1,0:T(8,128)(2,1)S(1)}, bf16[16,64,64]{2,1,0:T(8,128)(2,1)S(1)}, f32[16,64,64]{2,1,0:T(8,128)S(1)}, f32[16,64,64]{2,1,0:T(8,1...) custom-call(bf16[4,4,64,1024]{3,2,1,0:T(8,128)(2,1)} %bitcast.18, bf16[1024,128]{1,0:T(8,128)(2,1)} %wgt.1, ...), custom_call_target="tpu_custom_call" | custom-call | tf_op jit(solution)/shard_map/pallas_call | solution.py:511
  40.2 1.3 %shard_map.119 = (bf16[16,64,64]{2,1,0:T(8,128)(2,1)}, bf16[16,64,64]{2,1,0:T(8,128)(2,1)}, f32[16,64,64]{2,1,0:T(8,128)}, f32[16,64,64]{2,1,0:T(8,128)}, bf16[1...) custom-call(bf16[16,64,64]{2,1,0:T(8,128)(2,1)S(1)} %get-tuple-element.18.refs_0_, ...), custom_call_target="tpu_custom_call" | custom-call | tf_op jit(solution)/shard_map/pallas_call | solution.py:460

commit v5 on v4

--- a/solution.py
+++ b/solution.py
@@ -11,7 +11,8 @@
 MESH = pl.DeviceIdType.MESH
 CORES = 2
 INNER = 4
-PLACE = (0, 2, 1, 3)
+TAIL = 16
+GRAD, STATE = 0, 1
 FAR_FIRST = (2, 1, 3)
 OFFSETS = sorted(((dz, dy) for dz in range(4) for dy in range(4) if dz or dy),
                  key=lambda d: -sum(min(v, 4 - v) for v in d))
@@ -49,7 +50,7 @@
         return owner(r) * own + u
 
     def slot(r, u):
-        return u * inner + PLACE[r]
+        return u * inner + r
 
     def rows(r, u, count=1):
         return pl.ds(pl.multiple_of(slot(r, u) * length, length), count * length)
@@ -100,44 +101,38 @@
                       w_ss.at[0], w_rs.at[0], tp=to)
 
     def a_copy(kind, r, u):
-        return remote(a_out.at[u, kind, r - 1], a_in.at[u, kind, r], a_ss.at[0], a_rs.at[u],
+        return remote(a_out.at[kind, u, r - 1], a_in.at[kind, u, r], a_ss.at[0], a_rs.at[kind, u],
                       sp=z * inner + owner(r))
 
-    def e_copy(dz, dy):
-        return remote(e_out.at[lax.rem(y + dy, inner)], e_in.at[dz * inner + dy], e_ss.at[0], e_rs.at[0],
-                      sp=away(dz, dy))
-
-    def b_copy(side, r, u):
-        to = jnp.clip(z + r if side == 0 else z - r, 0, outer - 1)
-        return remote(b_out.at[side, u], b_in.at[side, u, r - 1], b_ss.at[0], b_rs.at[u],
-                      sp=to * inner + y)
-
-    def above(r):
-        return z + r < outer
-
-    def below(r):
-        return z >= r
-
-    def c_copy(side, r, u):
-        return remote(c_out.at[u, r, side], c_in.at[u, PLACE[r] - 1, side], c_ss.at[0],
-                      c_rs.at[u, PLACE[r] // 2], sp=z * inner + lax.rem(y - r + inner, inner))
+    def e_copy(r):
+        return remote(e_out.at[owner(r)], e_in.at[r], e_ss.at[0], e_rs.at[0], sp=z * inner + owner(r))
+
+    def b_part(ref, kind):
+        return ref if kind == GRAD else ref.at[pl.ds(0, dv)]
+
+    def b_copy(kind, r, u):
+        return remote(b_part(b_out.at[kind, u], kind), b_part(b_in.at[kind, u, r - 1], kind), b_ss.at[kind],
+                      b_rs.at[kind, u], sp=lax.rem(z + r, outer) * inner + y)
+
+    def c_copy(kind, r, u):
+        return remote(c_out.at[kind, u, r], c_in.at[kind, u, r - 1], c_ss.at[0], c_rs.at[kind, u],
+                      sp=z * inner + lax.rem(y - r + inner, inner))
 
     mate = x * CORES + 1 - core
 
     def d_copies(r, u, count):
-        at, half = rows(r, u, count), PLACE[r] // 2
+        at = rows(r, u, count)
         for k in FAR_FIRST:
-            remote(d_all.at[tpi, at], d_all.at[tpi, at], d_ss.at[0], d_rs.at[u, half],
+            remote(d_all.at[tpi, at], d_all.at[tpi, at], d_ss.at[0], d_rs.at[u],
                    tp=lax.rem(x + k, xs) * CORES + core).start()
         remote(d_all.at[tpi, at], d_all.at[tpi, at], f_ss.at[0], f_rs.at[u], tp=mate).start()
 
     def forward(u):
-        for half in range(2):
-            at = rows(half, u, 2)
-            take(d_all.at[pl.ds(0, xs - 1), at], d_rs.at[u, half])
-            for k in range(1, xs):
-                mine = d_all.at[lax.rem(x - k + xs, xs) * CORES + core, at]
-                remote(mine, mine, f_ss.at[0], f_rs.at[u], tp=mate).start()
+        at = rows(0, u, inner)
+        take(d_all.at[pl.ds(0, xs - 1), at], d_rs.at[u])
+        for k in range(1, xs):
+            mine = d_all.at[lax.rem(x - k + xs, xs) * CORES + core, at]
+            remote(mine, mine, f_ss.at[0], f_rs.at[u], tp=mate).start()
 
     def g_copy(dz, dy):
         to = away(dz, dy)
@@ -153,6 +148,7 @@
 
     sums, strict = matrix(lower, upper), matrix(row > col, row < col)
     left = lax.broadcasted_iota(jnp.int32, (length, pack), 1) < dk
+    tail_row = lax.broadcasted_iota(jnp.int32, (TAIL, pack), 0)
     left_tall = lax.broadcasted_iota(jnp.int32, (dv, pack), 1) < dk
 
     def directed(tri, blocks):
@@ -172,12 +168,6 @@
     def ends(c):
         return jnp.where(left[:1], c[length - 1:length], c[0:1])
 
-    for side in range(2):
-        for r in range(1, outer):
-            @pl.when(jnp.logical_not(below(r) if side == 0 else above(r)))
-            def _():
-                b_in[side, :, r - 1] = jnp.zeros((own, dv, pack), BF16)
-
     def decays(todo):
         blocks = [jnp.concatenate([decay_v[0, owner(r), u], decay_v[1, owner(r), u]], 1) for r, u in todo]
         made = directed(sums, blocks)
@@ -201,9 +191,9 @@
 
     def place(kind, r, u, value):
         if r == 0:
-            a_in[u, kind, 0] = value
+            a_in[kind, u, 0] = value
         else:
-            a_out[u, kind, r - 1] = value
+            a_out[kind, u, r - 1] = value
 
     def emit(kind, todo):
         kept, made = (grads if kind == 0 else states)(todo)
@@ -216,88 +206,98 @@
         at = rows(0, u, inner)
         val[at] = dot(hid_v[at], wgt_v[...]).astype(BF16)
 
-    everyone = tuple(range(inner))
+    everyone, visitors = tuple(range(inner)), tuple(range(1, inner))
+
+    def send(kind, u):
+        for r in FAR_FIRST:
+            a_copy(kind, r, u).start()
+
+    loaded(0, 1)
+    decays([(r, 0) for r in everyone])
+    emit(GRAD, [(r, 0) for r in visitors])
+    pl.semaphore_wait(barrier, sp + tp - 2)
+    send(GRAD, 0)
+    loaded(1, own - 1)
+    decays([(r, u) for u in range(1, own) for r in everyone])
+    for r in FAR_FIRST:
+        e_copy(r).start()
+    e_in[0] = e_out[y]
+    for u in range(1, own):
+        emit(GRAD, [(r, u) for r in visitors])
+        send(GRAD, u)
+
+    half_own, end = own // 2, own - 1
+    take(wgt_v, i_s.at[6])
+    take(k_v, i_s.at[7])
     for u in range(own):
-        todo = [(r, u) for r in FAR_FIRST]
-        if u == 0:
-            loaded(0, 1)
-            decays([(r, u) for r in everyone])
-        emit(0, todo)
-        if u == 0:
-            pl.semaphore_wait(barrier, sp + tp - 2)
-        for r, u in todo:
-            a_copy(0, r, u).start()
-        if u == 0:
-            loaded(1, own - 1)
-            decays([(r, n) for n in range(1, own) for r in everyone])
-            for offset in OFFSETS:
-                e_copy(*offset).start()
-            take(wgt_v, i_s.at[6])
-            take(k_v, i_s.at[7])
         take(hid_v.at[rows(0, u, inner)], h_s.at[u])
         values(u)
-        emit(1, todo)
-        for r, u in todo:
-            a_copy(1, r, u).start()
+        emit(STATE, [(r, u) for r in visitors])
+        if u < half_own:
+            send(STATE, u)
 
     for r in range(1, tp):
         w_copy(r).start()
     w_in[tpi] = wgt_v[pl.ds(pl.multiple_of(tpi * feat, feat), feat), :]
-    e_in[0] = e_out[y]
     mine = [(0, u) for u in range(own)]
-    emit(0, mine)
-    emit(1, mine)
+    emit(GRAD, mine)
+    emit(STATE, mine)
     w_acc[...] = jnp.zeros((dv, width), F32)
-
-    def ending(plane, person, u):
-        source = lax.rem(z - plane + outer, outer) * inner + lax.rem(y - person + inner, inner)
-        return e_in[source, pl.ds(u, 1), :]
-
-    people = (tuple(range(inner)), tuple(range(inner - 1, -1, -1)))
 
     def offset(person):
         return lax.rem(y - person + inner, inner)
 
-    def combine_plane(u):
-        take(a_in.at[u, :, pl.ds(1, inner - 1)], a_rs.at[u])
-        for side in range(2):
-            running = jnp.zeros((dv, pack), F32)
-            for n, person in enumerate(people[side]):
-                grad, state = a_in[u, 0, offset(person)], a_in[u, 1, offset(person)]
-                block = jnp.where(left_tall, state, grad) if side == 0 else jnp.where(left_tall, grad, state)
-                if n == 0:
-                    running = block.astype(F32)
-                else:
-                    local[side, person, u] = running
-                    running = jnp.exp(ending(z, person, u)) * running + block.astype(F32)
-            b_out[side, u] = running.astype(BF16)
-        for side in range(2):
-            for r in range(1, outer):
-                @pl.when(above(r) if side == 0 else below(r))
-                def _():
-                    b_copy(side, r, u).start()
-
-    def combine_all(u):
-        take(b_in.at[0, u], b_rs.at[u])
-        for side in range(2):
-            carried = b_in[side, u, 0].astype(F32)
-            passed = jnp.zeros((1, pack), F32)
-            for r in range(2, outer):
-                plane = lax.rem(z - r + 1 + outer, outer) if side == 0 else lax.rem(z + r - 1, outer)
-                for person in range(inner):
-                    passed = passed + ending(plane, person, u)
-                carried = carried + jnp.exp(passed) * b_in[side, u, r - 1].astype(F32)
-            passed = jnp.zeros((1, pack), F32)
-            for n, person in enumerate(people[side]):
-                if n == 0:
-                    c_out[u, offset(person), side] = carried.astype(BF16)
-                else:
-                    out = jnp.exp(passed) * carried + local[side, person, u]
-                    c_out[u, offset(person), side] = out.astype(BF16)
-                passed = passed + ending(z, person, u)
+    def endings(u):
+        return [e_in[offset(person), pl.ds(u, 1), :] for person in everyone]
+
+    def pick(kind, ahead, behind):
+        at = left_tall if ahead.shape[0] == dv else left[:1]
+        return jnp.where(at, ahead, behind) if kind == STATE else jnp.where(at, behind, ahead)
+
+    def running(blocks, factors, order):
+        total, before = None, [None] * inner
+        for person in order:
+            before[person] = jnp.zeros((dv, pack), F32) if total is None else total
+            total = blocks[person] if total is None else factors[person] * total + blocks[person]
+        return before, total
+
+    def combine_plane(kind, u):
+        take(a_in.at[kind, u, pl.ds(1, inner - 1)], a_rs.at[kind, u])
+        blocks = [a_in[kind, u, offset(person)].astype(F32) for person in everyone]
+        ends_ = endings(u)
+        factors = [jnp.exp(e) for e in ends_]
+        before, total = running(blocks, factors, everyone)
+        after, total_back = running(blocks, factors, everyone[::-1])
+        for person in everyone:
+            local[kind, u, person] = pick(kind, before[person], after[person])
+        b_out[kind, u, pl.ds(0, dv)] = pick(kind, total, total_back).astype(BF16)
+        if kind == GRAD:
+            whole = sum(ends_[1:], ends_[0])
+            high = whole.astype(BF16).astype(F32)
+            tail = jnp.where(tail_row == 0, high, jnp.where(tail_row == 1, whole - high, 0.0))
+            b_out[kind, u, pl.ds(dv, TAIL)] = tail.astype(BF16)
         for r in FAR_FIRST:
-            for side in range(2):
-                c_copy(side, r, u).start()
+            b_copy(kind, r, u).start()
+
+    def combine_all(kind, u):
+        take(b_in.at[GRAD, u] if kind == GRAD else b_in.at[STATE, u, :, pl.ds(0, dv)], b_rs.at[kind, u])
+        planes = [None]
+        for r in range(1, outer):
+            tail = b_in[GRAD, u, r - 1, pl.ds(dv, TAIL)].astype(F32)
+            planes.append(tail[0:1] + tail[1:2])
+        zero = jnp.zeros((1, pack), F32)
+        carried = jnp.zeros((dv, pack), F32)
+        for r in range(1, outer):
+            q = outer - r
+            ahead = jnp.where(z >= r, jnp.exp(sum(planes[1:r], zero)), 0.0)
+            behind = jnp.where(z + q < outer, jnp.exp(sum(planes[r + 1:], zero)), 0.0)
+            carried = carried + pick(kind, ahead, behind) * b_in[kind, u, r - 1, pl.ds(0, dv)].astype(F32)
+        ends_ = endings(u)
+        for person in everyone:
+            factor = jnp.exp(pick(kind, sum(ends_[:person], zero), sum(ends_[person + 1:], zero)))
+            c_out[kind, u, offset(person)] = (factor * carried + local[kind, u, person]).astype(BF16)
+        for r in FAR_FIRST:
+            c_copy(kind, r, u).start()
 
     def intra(todo):
         made = []
@@ -322,12 +322,11 @@
             intra_k[slot(r, u)] = for_k
             intra_v[slot(r, u)] = for_v
 
-    def arrived(r, u):
-        low, up = (c_out[u, 0, 0], c_out[u, 0, 1]) if r == 0 else (c_in[u, PLACE[r] - 1, 0], c_in[u, PLACE[r] - 1, 1])
-        return jnp.where(left_tall, low, up), jnp.where(left_tall, up, low)
+    def arrived(kind, r, u):
+        return c_out[kind, u, 0] if r == 0 else c_in[kind, u, r - 1]
 
     def finish_values(todo):
-        made = [intra_v[slot(r, u)] + dot(k_ends[slot(r, u)], arrived(r, u)[1], 1, 1) for r, u in todo]
+        made = [intra_v[slot(r, u)] + dot(k_ends[slot(r, u)], arrived(GRAD, r, u), 1, 1) for r, u in todo]
         for (r, u), block in zip(todo, made):
             d_all[tpi, rows(r, u)] = block.astype(BF16)
 
@@ -335,7 +334,7 @@
         kept, terms = [], []
         for r, u in todo:
             s = slot(r, u)
-            state, grad = arrived(r, u)
+            state, grad = arrived(STATE, r, u), arrived(GRAD, r, u)
             c = cum[s]
             end = ends(c)
             grow, shrink, to_end = jnp.exp(c), jnp.exp(-c), jnp.exp(end - c)
@@ -355,11 +354,6 @@
             o_f[b] = decay_grad[:, :dk]
             o_b[b] = decay_grad[:, dk:]
 
-    def finish_own(u):
-        finish_values([(0, u)])
-        d_copies(0, u, 1)
-        finish_rest([(0, u)])
-
     def features(u):
         take(d_all.at[pl.ds(0, xs), rows(0, u, inner)], f_rs.at[u])
         at = rows(0, u, inner)
@@ -367,68 +361,86 @@
         weights = jnp.concatenate([w_in[t] for t in range(tp)], 1)
         out = dot(wide, weights, 1, 1).astype(BF16)
         for r in range(inner):
-            o_h[batch_of(r, u)] = out[PLACE[r] * length:(PLACE[r] + 1) * length]
-
-    def finish_others(todo, u):
-        first = PLACE[todo[0]] - 1
-        take(c_in.at[u, pl.ds(first, len(todo))], c_rs.at[u, (first + 1) // 2])
-        todo = [(r, u) for r in todo]
-        finish_values(todo)
-        d_copies(*todo[0], len(todo))
-
-    def weight_terms(r, u):
-        at = rows(r, u, 2)
+            o_h[batch_of(r, u)] = out[r * length:(r + 1) * length]
+
+    def finish_own(u):
+        finish_values([(0, u)])
+        d_copies(0, u, 1)
+
+    def finish_others(u):
+        take(c_in.at[GRAD, u], c_rs.at[GRAD, u])
+        finish_values([(r, u) for r in visitors])
+        d_copies(1, u, inner - 1)
+
+    def weight_terms(u):
+        at = rows(0, u, inner)
         return dot(d_all[tpi, at], hid_v[at], 0, 0)
 
-    def others(u):
-        finish_others([2], u)
-        finish_others([1, 3], u)
-        at = rows(0, u, inner)
-        w_acc[...] += dot(d_all[tpi, at], hid_v[at], 0, 0)
-        finish_rest([(r, u) for r in range(1, inner)])
+    def rest_others(u):
+        take(c_in.at[STATE, u], c_rs.at[STATE, u])
+        finish_rest([(r, u) for r in visitors])
 
     def loop(first, last, step):
         lax.fori_loop(first, last, lambda u, _: step(u) or 0, 0)
 
     def intra_all(u):
-        intra([(r, u) for r in range(inner)])
-
-    def middle_steps(u):
-        combine_all(u)
+        intra([(r, u) for r in everyone])
+
+    def first_steps(u):
+        combine_plane(GRAD, u)
+        intra_all(u)
+
+    def second_steps(u):
+        combine_all(GRAD, u)
         finish_own(u)
-        combine_plane(u + half_own)
-
-    def late_steps(u):
-        combine_all(u)
-        finish_own(u)
-        others(u - half_own)
-
-    half_own, end = own // 2, own - 1
-    loop(0, half_own, intra_all)
-    take(e_in.at[pl.ds(1, sp - 1)], e_rs.at[0])
-    combine_plane(0)
-    loop(half_own, own, intra_all)
-    loop(1, half_own, combine_plane)
-    loop(0, half_own, middle_steps)
-    loop(half_own, own, late_steps)
-    loop(half_own, end, others)
-
-    finish_others([2], end)
-    w_acc[...] += weight_terms(0, end)
-    finish_others([1, 3], end)
-    full = w_acc[...] + weight_terms(1, end)
+
+        @pl.when(u < end)
+        def _():
+            combine_plane(STATE, u - 1)
+
+    def weigh(u):
+        finish_others(u)
+        w_acc[...] += weight_terms(u)
+
+    def third_steps(u):
+        weigh(u)
+        combine_all(STATE, u)
+        finish_rest([(0, u)])
+
+    def fourth_steps(u):
+        forward(u)
+        rest_others(u)
+        combine_all(STATE, u + half_own)
+        finish_rest([(0, u + half_own)])
+
+    take(e_in.at[pl.ds(1, inner - 1)], e_rs.at[0])
+    loop(0, end, first_steps)
+    combine_plane(GRAD, end)
+    combine_all(GRAD, 0)
+    finish_own(0)
+    intra_all(end)
+    loop(1, own, second_steps)
+    loop(half_own, own, lambda u: send(STATE, u))
+    loop(0, half_own, third_steps)
+    loop(half_own, end, weigh)
+
+    finish_others(end)
+    full = w_acc[...] + weight_terms(end)
     for p in range(0, sp, 2):
         block = full[:, p * rows_sp:(p + 2) * rows_sp].T.astype(BF16)
         g_out[p] = block[:rows_sp]
         g_out[p + 1] = block[rows_sp:]
-    for offset in OFFSETS:
-        g_copy(*offset).start()
-    finish_rest([(r, end) for r in range(1, inner)])
-    loop(0, end, forward)
+    for away_by in OFFSETS:
+        g_copy(*away_by).start()
+
+    loop(half_own, own, lambda u: combine_plane(STATE, u))
+    loop(0, half_own, fourth_steps)
+    loop(half_own, own, forward)
     take(w_in.at[pl.ds(0, tp - 1)], w_rs.at[0])
-    loop(0, half_own, features)
-    forward(end)
-    loop(half_own, own, features)
+    loop(0, end, features)
+    loop(half_own, end, rest_others)
+    features(end)
+    rest_others(end)
 
     take(g_in, g_rs.at[0])
     acc = g_out[spi].astype(F32)
@@ -437,9 +449,10 @@
     o_w[...] = acc
 
     take(w_in.at[pl.ds(0, tp - 1)], w_ss.at[0])
-    take(e_in.at[pl.ds(1, sp - 1)], e_ss.at[0])
+    take(e_in.at[pl.ds(1, inner - 1)], e_ss.at[0])
     take(a_out, a_ss.at[0])
-    take(b_in.at[0], b_ss.at[0])
+    take(b_in.at[GRAD], b_ss.at[GRAD])
+    take(b_in.at[STATE, :, :, pl.ds(0, dv)], b_ss.at[STATE])
     take(c_in, c_ss.at[0])
     take(d_all.at[pl.ds(0, xs - 1)], d_ss.at[0])
     take(d_all.at[pl.ds(0, xs)], f_ss.at[0])
@@ -485,20 +498,20 @@
         vmem((batch, length, pack), BF16), vmem((batch, length, pack), BF16),
         vmem((batch, length, pack), F32), vmem((batch, length, pack), F32),
         vmem((batch, length, dv), F32),
-        vmem((own, 2, inner - 1, dv, pack), BF16), vmem((own, 2, inner, dv, pack), BF16),
-        vmem((inner, own, pack), F32), vmem((sp, own, pack), F32),
-        vmem((2, inner, own, dv, pack), F32),
-        vmem((2, own, dv, pack), BF16), vmem((2, own, outer - 1, dv, pack), BF16),
-        vmem((own, inner, 2, dv, pack), BF16), vmem((own, inner - 1, 2, dv, pack), BF16),
+        vmem((2, own, inner - 1, dv, pack), BF16), vmem((2, own, inner, dv, pack), BF16),
+        vmem((inner, own, pack), F32), vmem((inner, own, pack), F32),
+        vmem((2, own, inner, dv, pack), F32),
+        vmem((2, own, dv + TAIL, pack), BF16), vmem((2, own, outer - 1, dv + TAIL, pack), BF16),
+        vmem((2, own, inner, dv, pack), BF16), vmem((2, own, inner - 1, dv, pack), BF16),
         vmem((tp, rows, dv), BF16), vmem((tp, feat, dv), BF16),
         vmem((dv, width), F32),
         vmem((sp, rows_sp, dv), BF16), vmem((sp - 1, rows_sp, dv), BF16),
         dma((8,)), dma((own,)),
+        dma((1,)), dma((2, own)),
+        dma((1,)), dma((1,)),
+        dma((2,)), dma((2, own)),
+        dma((1,)), dma((2, own)),
         dma((1,)), dma((own,)),
-        dma((1,)), dma((1,)),
-        dma((1,)), dma((own,)),
-        dma((1,)), dma((own, 2)),
-        dma((1,)), dma((own, 2)),
         dma((1,)), dma((own,)),
         dma((1,)), dma((1,)),
         dma((1,)), dma((1,)),

time: 41.6 us -> 40.2 us (0.966)
  Pallas kernels: 40.8 us -> 39.5 us
    pallas_call x1, Pallas kernels: 39.5 us -> 38.2 us  [shards(): pl.pallas_call(functools.partial(kernel, dims), out_shape=(vmem(flat, BF1...]
where the time goes in v5:
time: 40.2 us; the launch traced here: 40.1 us
  Pallas kernels  39.5 us (98%)
  between operations  0.64 us (2%)
    pallas_call x1, Pallas kernels, shards(): pl.pallas_call(functools.partial(kernel, dims), out_shape=(vmem(flat, BF1...  38.2 us
    pallas_call x1, Pallas kernels, store(): pl.pallas_call(store_kernel, out_shape=tuple((jax.ShapeDtypeStruct(a.shap...  1.28 us

profile of v5, /device:TPU:1, one launch (start us, length us, event | category | flops | bytes accessed | tf_op | source)
XLA Modules:
  0.0 40.1 jit_solution(8993999228809981052)
XLA Ops:
  0.6 38.2 %shard_map.118 = (bf16[16,64,64]{2,1,0:T(8,128)(2,1)S(1)}, bf16[16,64,64]{2,1,0:T(8,128)(2,1)S(1)}, f32[16,64,64]{2,1,0:T(8,128)S(1)}, f32[16,64,64]{2,1,0:T(8,1...) custom-call(bf16[4,4,64,1024]{3,2,1,0:T(8,128)(2,1)} %bitcast.18, bf16[1024,128]{1,0:T(8,128)(2,1)} %wgt.1, ...), custom_call_target="tpu_custom_call" | custom-call | tf_op jit(solution)/shard_map/pallas_call | solution.py:524
  38.8 1.3 %shard_map.119 = (bf16[16,64,64]{2,1,0:T(8,128)(2,1)}, bf16[16,64,64]{2,1,0:T(8,128)(2,1)}, f32[16,64,64]{2,1,0:T(8,128)}, f32[16,64,64]{2,1,0:T(8,128)}, bf16[1...) custom-call(bf16[16,64,64]{2,1,0:T(8,128)(2,1)S(1)} %get-tuple-element.18.refs_0_, ...), custom_call_target="tpu_custom_call" | custom-call | tf_op jit(solution)/shard_map/pallas_call | solution.py:473

commit v6 on v5

--- a/solution.py
+++ b/solution.py
@@ -226,14 +226,14 @@
         emit(GRAD, [(r, u) for r in visitors])
         send(GRAD, u)
 
-    half_own, end = own // 2, own - 1
+    end = own - 1
     take(wgt_v, i_s.at[6])
     take(k_v, i_s.at[7])
     for u in range(own):
         take(hid_v.at[rows(0, u, inner)], h_s.at[u])
         values(u)
         emit(STATE, [(r, u) for r in visitors])
-        if u < half_own:
+        if u < end:
             send(STATE, u)
 
     for r in range(1, tp):
@@ -393,36 +393,36 @@
     def second_steps(u):
         combine_all(GRAD, u)
         finish_own(u)
-
-        @pl.when(u < end)
-        def _():
-            combine_plane(STATE, u - 1)
+        combine_plane(STATE, u - 1)
 
     def weigh(u):
         finish_others(u)
         w_acc[...] += weight_terms(u)
 
+    def pass_states(u):
+        combine_all(STATE, u)
+        finish_rest([(0, u)])
+
     def third_steps(u):
         weigh(u)
-        combine_all(STATE, u)
-        finish_rest([(0, u)])
+        pass_states(u)
 
     def fourth_steps(u):
         forward(u)
         rest_others(u)
-        combine_all(STATE, u + half_own)
-        finish_rest([(0, u + half_own)])
 
     take(e_in.at[pl.ds(1, inner - 1)], e_rs.at[0])
     loop(0, end, first_steps)
     combine_plane(GRAD, end)
     combine_all(GRAD, 0)
+    send(STATE, end)
     finish_own(0)
     intra_all(end)
     loop(1, own, second_steps)
-    loop(half_own, own, lambda u: send(STATE, u))
-    loop(0, half_own, third_steps)
-    loop(half_own, end, weigh)
+    weigh(0)
+    combine_plane(STATE, end)
+    pass_states(0)
+    loop(1, end, third_steps)
 
     finish_others(end)
     full = w_acc[...] + weight_terms(end)
@@ -433,14 +433,13 @@
     for away_by in OFFSETS:
         g_copy(*away_by).start()
 
-    loop(half_own, own, lambda u: combine_plane(STATE, u))
-    loop(0, half_own, fourth_steps)
-    loop(half_own, own, forward)
+    pass_states(end)
+    loop(0, end, fourth_steps)
+    forward(end)
     take(w_in.at[pl.ds(0, tp - 1)], w_rs.at[0])
     loop(0, end, features)
-    loop(half_own, end, rest_others)
+    rest_others(end)
     features(end)
-    rest_others(end)
 
     take(g_in, g_rs.at[0])
     acc = g_out[spi].astype(F32)

time: 40.2 us -> 38 us (0.945)
  Pallas kernels: 39.5 us -> 37.3 us
    pallas_call x1, Pallas kernels: 38.2 us -> 36 us  [shards(): pl.pallas_call(functools.partial(kernel, dims), out_shape=(vmem(flat, BF1...]
where the time goes in v6:
time: 38 us; the launch traced here: 37.9 us
  Pallas kernels  37.3 us (98%)
  between operations  0.64 us (2%)
    pallas_call x1, Pallas kernels, shards(): pl.pallas_call(functools.partial(kernel, dims), out_shape=(vmem(flat, BF1...  36 us
    pallas_call x1, Pallas kernels, store(): pl.pallas_call(store_kernel, out_shape=tuple((jax.ShapeDtypeStruct(a.shap...  1.28 us

profile of v6, /device:TPU:1, one launch (start us, length us, event | category | flops | bytes accessed | tf_op | source)
XLA Modules:
  0.0 37.9 jit_solution(7822205396544520203)
XLA Ops:
  0.6 36.0 %shard_map.118 = (bf16[16,64,64]{2,1,0:T(8,128)(2,1)S(1)}, bf16[16,64,64]{2,1,0:T(8,128)(2,1)S(1)}, f32[16,64,64]{2,1,0:T(8,128)S(1)}, f32[16,64,64]{2,1,0:T(8,1...) custom-call(bf16[4,4,64,1024]{3,2,1,0:T(8,128)(2,1)} %bitcast.18, bf16[1024,128]{1,0:T(8,128)(2,1)} %wgt.1, ...), custom_call_target="tpu_custom_call" | custom-call | tf_op jit(solution)/shard_map/pallas_call | solution.py:523
  36.6 1.3 %shard_map.119 = (bf16[16,64,64]{2,1,0:T(8,128)(2,1)}, bf16[16,64,64]{2,1,0:T(8,128)(2,1)}, f32[16,64,64]{2,1,0:T(8,128)}, f32[16,64,64]{2,1,0:T(8,128)}, bf16[1...) custom-call(bf16[16,64,64]{2,1,0:T(8,128)(2,1)S(1)} %get-tuple-element.18.refs_0_, ...), custom_call_target="tpu_custom_call" | custom-call | tf_op jit(solution)/shard_map/pallas_call | solution.py:472

commit v7 on v6

--- a/solution.py
+++ b/solution.py
@@ -38,6 +38,7 @@
     sp, tp, batch, length, dk, dv, width = dims
     inner, outer, own, xs = INNER, sp // INNER, batch // INNER, tp // CORES
     pack, feat, rows_sp, group = 2 * dk, width // tp, width // sp, INNER * length
+    fold = dv // 2
     spi, tpi = lax.axis_index("sp"), lax.axis_index("tp")
     z, y = spi // inner, lax.rem(spi, inner)
     x, core = tpi // CORES, lax.rem(tpi, CORES)
@@ -79,8 +80,10 @@
             pltpu.make_async_copy(hid.at[owner(r), u], hid_v.at[rows(r, u)], h_s.at[u]).start()
 
     load(0, 1)
-    for r in range(1, sp):
-        pl.semaphore_signal(barrier, inc=1, device_id={"sp": lax.rem(spi + r, sp)}, device_id_type=MESH)
+    for r in range(1, outer):
+        pl.semaphore_signal(barrier, inc=1, device_id={"sp": away(r, 0)}, device_id_type=MESH)
+    for r in range(1, inner):
+        pl.semaphore_signal(barrier, inc=1, device_id={"sp": away(0, r)}, device_id_type=MESH)
     for r in range(1, tp):
         pl.semaphore_signal(barrier, inc=1, device_id={"tp": lax.rem(tpi + r, tp)}, device_id_type=MESH)
 
@@ -108,11 +111,12 @@
         return remote(e_out.at[owner(r)], e_in.at[r], e_ss.at[0], e_rs.at[0], sp=z * inner + owner(r))
 
     def b_part(ref, kind):
-        return ref if kind == GRAD else ref.at[pl.ds(0, dv)]
+        return ref if kind == GRAD else ref.at[pl.ds(0, fold)]
 
     def b_copy(kind, r, u):
-        return remote(b_part(b_out.at[kind, u], kind), b_part(b_in.at[kind, u, r - 1], kind), b_ss.at[kind],
-                      b_rs.at[kind, u], sp=lax.rem(z + r, outer) * inner + y)
+        way = jnp.where(z + r < outer, 0, 1)
+        return remote(b_part(b_out.at[kind, u, way], kind), b_part(b_in.at[kind, u, r - 1], kind),
+                      b_ss.at[kind], b_rs.at[kind, u], sp=lax.rem(z + r, outer) * inner + y)
 
     def c_copy(kind, r, u):
         return remote(c_out.at[kind, u, r], c_in.at[kind, u, r - 1], c_ss.at[0], c_rs.at[kind, u],
@@ -148,6 +152,7 @@
 
     sums, strict = matrix(lower, upper), matrix(row > col, row < col)
     left = lax.broadcasted_iota(jnp.int32, (length, pack), 1) < dk
+    left_fold = lax.broadcasted_iota(jnp.int32, (fold, pack), 1) < dk
     tail_row = lax.broadcasted_iota(jnp.int32, (TAIL, pack), 0)
     left_tall = lax.broadcasted_iota(jnp.int32, (dv, pack), 1) < dk
 
@@ -215,7 +220,7 @@
     loaded(0, 1)
     decays([(r, 0) for r in everyone])
     emit(GRAD, [(r, 0) for r in visitors])
-    pl.semaphore_wait(barrier, sp + tp - 2)
+    pl.semaphore_wait(barrier, inner + outer + tp - 3)
     send(GRAD, 0)
     loaded(1, own - 1)
     decays([(r, u) for u in range(1, own) for r in everyone])
@@ -254,6 +259,18 @@
         at = left_tall if ahead.shape[0] == dv else left[:1]
         return jnp.where(at, ahead, behind) if kind == STATE else jnp.where(at, behind, ahead)
 
+    def turn(v):
+        return pltpu.roll(v, dk, 1)
+
+    def folded(v, first):
+        if first:
+            return jnp.where(left_fold, v[:fold], turn(v[fold:]))
+        return jnp.where(left_fold, turn(v[:fold]), v[fold:])
+
+    def unfolded(first, second):
+        return jnp.concatenate([jnp.where(left_fold, first, turn(second)),
+                                jnp.where(left_fold, turn(first), second)], 0)
+
     def running(blocks, factors, order):
         total, before = None, [None] * inner
         for person in order:
@@ -270,28 +287,33 @@
         after, total_back = running(blocks, factors, everyone[::-1])
         for person in everyone:
             local[kind, u, person] = pick(kind, before[person], after[person])
-        b_out[kind, u, pl.ds(0, dv)] = pick(kind, total, total_back).astype(BF16)
+        b_out[kind, u, 0, pl.ds(0, fold)] = folded(total, kind == STATE).astype(BF16)
+        b_out[kind, u, 1, pl.ds(0, fold)] = folded(total_back, kind == GRAD).astype(BF16)
         if kind == GRAD:
             whole = sum(ends_[1:], ends_[0])
             high = whole.astype(BF16).astype(F32)
-            tail = jnp.where(tail_row == 0, high, jnp.where(tail_row == 1, whole - high, 0.0))
-            b_out[kind, u, pl.ds(dv, TAIL)] = tail.astype(BF16)
+            tail = jnp.where(tail_row == 0, high, jnp.where(tail_row == 1, whole - high, 0.0)).astype(BF16)
+            for way in range(2):
+                b_out[kind, u, way, pl.ds(fold, TAIL)] = tail
         for r in FAR_FIRST:
             b_copy(kind, r, u).start()
 
     def combine_all(kind, u):
-        take(b_in.at[GRAD, u] if kind == GRAD else b_in.at[STATE, u, :, pl.ds(0, dv)], b_rs.at[kind, u])
+        take(b_in.at[GRAD, u] if kind == GRAD else b_in.at[STATE, u, :, pl.ds(0, fold)], b_rs.at[kind, u])
         planes = [None]
         for r in range(1, outer):
-            tail = b_in[GRAD, u, r - 1, pl.ds(dv, TAIL)].astype(F32)
+            tail = b_in[GRAD, u, r - 1, pl.ds(fold, TAIL)].astype(F32)
             planes.append(tail[0:1] + tail[1:2])
         zero = jnp.zeros((1, pack), F32)
-        carried = jnp.zeros((dv, pack), F32)
+        ahead, behind = jnp.zeros((fold, pack), F32), jnp.zeros((fold, pack), F32)
         for r in range(1, outer):
-            q = outer - r
-            ahead = jnp.where(z >= r, jnp.exp(sum(planes[1:r], zero)), 0.0)
-            behind = jnp.where(z + q < outer, jnp.exp(sum(planes[r + 1:], zero)), 0.0)
-            carried = carried + pick(kind, ahead, behind) * b_in[kind, u, r - 1, pl.ds(0, dv)].astype(F32)
+            block = b_in[kind, u, r - 1, pl.ds(0, fold)].astype(F32)
+            passed, back = sum(planes[1:r], zero), sum(planes[r + 1:], zero)
+            first = jnp.where(left[:1], passed, turn(passed)) if kind == STATE else jnp.where(left[:1], turn(passed), passed)
+            second = jnp.where(left[:1], back, turn(back)) if kind == GRAD else jnp.where(left[:1], turn(back), back)
+            ahead = ahead + jnp.where(z >= r, jnp.exp(first), 0.0) * block
+            behind = behind + jnp.where(z + outer - r < outer, jnp.exp(second), 0.0) * block
+        carried = unfolded(ahead, behind) if kind == STATE else unfolded(behind, ahead)
         ends_ = endings(u)
         for person in everyone:
             factor = jnp.exp(pick(kind, sum(ends_[:person], zero), sum(ends_[person + 1:], zero)))
@@ -415,14 +437,13 @@
     loop(0, end, first_steps)
     combine_plane(GRAD, end)
     combine_all(GRAD, 0)
-    send(STATE, end)
     finish_own(0)
     intra_all(end)
-    loop(1, own, second_steps)
-    weigh(0)
+    loop(1, end, second_steps)
+    send(STATE, end)
+    second_steps(end)
+    loop(0, end, third_steps)
     combine_plane(STATE, end)
-    pass_states(0)
-    loop(1, end, third_steps)
 
     finish_others(end)
     full = w_acc[...] + weight_terms(end)
@@ -432,14 +453,14 @@
         g_out[p + 1] = block[rows_sp:]
     for away_by in OFFSETS:
         g_copy(*away_by).start()
-
+    loop(0, end - 1, fourth_steps)
+    forward(end - 1)
     pass_states(end)
-    loop(0, end, fourth_steps)
     forward(end)
+    rest_others(end - 1)
     take(w_in.at[pl.ds(0, tp - 1)], w_rs.at[0])
-    loop(0, end, features)
+    loop(0, own, features)
     rest_others(end)
-    features(end)
 
     take(g_in, g_rs.at[0])
     acc = g_out[spi].astype(F32)
@@ -451,7 +472,7 @@
     take(e_in.at[pl.ds(1, inner - 1)], e_ss.at[0])
     take(a_out, a_ss.at[0])
     take(b_in.at[GRAD], b_ss.at[GRAD])
-    take(b_in.at[STATE, :, :, pl.ds(0, dv)], b_ss.at[STATE])
+    take(b_in.at[STATE, :, :, pl.ds(0, fold)], b_ss.at[STATE])
     take(c_in, c_ss.at[0])
     take(d_all.at[pl.ds(0, xs - 1)], d_ss.at[0])
     take(d_all.at[pl.ds(0, xs)], f_ss.at[0])
@@ -500,7 +521,7 @@
         vmem((2, own, inner - 1, dv, pack), BF16), vmem((2, own, inner, dv, pack), BF16),
         vmem((inner, own, pack), F32), vmem((inner, own, pack), F32),
         vmem((2, own, inner, dv, pack), F32),
-        vmem((2, own, dv + TAIL, pack), BF16), vmem((2, own, outer - 1, dv + TAIL, pack), BF16),
+        vmem((2, own, 2, dv // 2 + TAIL, pack), BF16), vmem((2, own, outer - 1, dv // 2 + TAIL, pack), BF16),
         vmem((2, own, inner, dv, pack), BF16), vmem((2, own, inner - 1, dv, pack), BF16),
         vmem((tp, rows, dv), BF16), vmem((tp, feat, dv), BF16),
         vmem((dv, width), F32),

time: 38 us -> 37.6 us (0.989)
  the two profiles are of different devices: /device:TPU:1 before, /device:TPU:0 now
where the time goes in v7:
time: 37.6 us; the launch traced here: 37.5 us
  Pallas kernels  36.9 us (98%)
  between operations  0.64 us (2%)
    pallas_call x1, Pallas kernels, shards(): pl.pallas_call(functools.partial(kernel, dims), out_shape=(vmem(flat, BF1...  35.6 us
    pallas_call x1, Pallas kernels, store(): pl.pallas_call(store_kernel, out_shape=tuple((jax.ShapeDtypeStruct(a.shap...  1.28 us

profile of v7, /device:TPU:0, one launch (start us, length us, event | category | flops | bytes accessed | tf_op | source)
XLA Modules:
  0.0 37.5 jit_solution(8107991919885988539)
XLA Ops:
  0.6 35.6 %shard_map.118 = (bf16[16,64,64]{2,1,0:T(8,128)(2,1)S(1)}, bf16[16,64,64]{2,1,0:T(8,128)(2,1)S(1)}, f32[16,64,64]{2,1,0:T(8,128)S(1)}, f32[16,64,64]{2,1,0:T(8,1...) custom-call(bf16[4,4,64,1024]{3,2,1,0:T(8,128)(2,1)} %bitcast.18, bf16[1024,128]{1,0:T(8,128)(2,1)} %wgt.1, ...), custom_call_target="tpu_custom_call" | custom-call | tf_op jit(solution)/shard_map/pallas_call | solution.py:544
  36.3 1.3 %shard_map.119 = (bf16[16,64,64]{2,1,0:T(8,128)(2,1)}, bf16[16,64,64]{2,1,0:T(8,128)(2,1)}, f32[16,64,64]{2,1,0:T(8,128)}, f32[16,64,64]{2,1,0:T(8,128)}, bf16[1...) custom-call(bf16[16,64,64]{2,1,0:T(8,128)(2,1)S(1)} %get-tuple-element.18.refs_0_, ...), custom_call_target="tpu_custom_call" | custom-call | tf_op jit(solution)/shard_map/pallas_call | solution.py:493

commit v8 on v7

--- a/solution.py
+++ b/solution.py
@@ -44,6 +44,8 @@
     x, core = tpi // CORES, lax.rem(tpi, CORES)
 
     barrier = pltpu.get_barrier_semaphore()
+    mate = x * CORES + 1 - core
+    inside = (x > 0) & (x < xs - 1)
     def owner(r):
         return lax.rem(y + r, inner)
 
@@ -84,8 +86,13 @@
         pl.semaphore_signal(barrier, inc=1, device_id={"sp": away(r, 0)}, device_id_type=MESH)
     for r in range(1, inner):
         pl.semaphore_signal(barrier, inc=1, device_id={"sp": away(0, r)}, device_id_type=MESH)
-    for r in range(1, tp):
-        pl.semaphore_signal(barrier, inc=1, device_id={"tp": lax.rem(tpi + r, tp)}, device_id_type=MESH)
+    pl.semaphore_signal(barrier, inc=1, device_id={"tp": mate}, device_id_type=MESH)
+    for step in (1, -1):
+        @pl.when((x + step >= 0) & (x + step < xs))
+        def _():
+            for c in range(CORES):
+                pl.semaphore_signal(barrier, inc=1, device_id={"tp": jnp.clip(x + step, 0, xs - 1) * CORES + c},
+                                    device_id_type=MESH)
 
     pltpu.make_async_copy(wgt, wgt_v, i_s.at[6]).start()
     load_hidden(0)
@@ -98,10 +105,33 @@
         return pltpu.make_async_remote_copy(src_ref=src, dst_ref=dst, send_sem=ss, recv_sem=rs,
                                             device_id=where, device_id_type=MESH)
 
-    def w_copy(r):
-        to = lax.rem(tpi + r, tp)
+    def w_copy(to, phase):
         return remote(wgt_v.at[pl.ds(pl.multiple_of(to * feat, feat), feat), :], w_in.at[tpi],
-                      w_ss.at[0], w_rs.at[0], tp=to)
+                      w_ss.at[0], w_rs.at[phase], tp=to)
+
+    def w_near():
+        w_copy(mate, 0).start()
+        for step in (1, -1):
+            @pl.when((x + step >= 0) & (x + step < xs))
+            def _():
+                for c in range(CORES):
+                    w_copy(jnp.clip(x + step, 0, xs - 1) * CORES + c, 0).start()
+
+    def w_across():
+        for many in range(2):
+            @pl.when(inside if many else jnp.logical_not(inside))
+            def _():
+                take(w_in.at[pl.ds(0, 1 + CORES * (1 + many))], w_rs.at[0])
+        for c in range(CORES):
+            w_copy(lax.rem(x + 2, xs) * CORES + c, 1).start()
+
+    def w_ends():
+        take(w_in.at[pl.ds(0, CORES)], w_rs.at[1])
+
+        @pl.when(jnp.logical_not(inside))
+        def _():
+            for c in range(CORES):
+                w_copy((xs - 1 - x) * CORES + c, 2).start()
 
     def a_copy(kind, r, u):
         return remote(a_out.at[kind, u, r - 1], a_in.at[kind, u, r], a_ss.at[0], a_rs.at[kind, u],
@@ -121,8 +151,6 @@
     def c_copy(kind, r, u):
         return remote(c_out.at[kind, u, r], c_in.at[kind, u, r - 1], c_ss.at[0], c_rs.at[kind, u],
                       sp=z * inner + lax.rem(y - r + inner, inner))
-
-    mate = x * CORES + 1 - core
 
     def d_copies(r, u, count):
         at = rows(r, u, count)
@@ -220,7 +248,7 @@
     loaded(0, 1)
     decays([(r, 0) for r in everyone])
     emit(GRAD, [(r, 0) for r in visitors])
-    pl.semaphore_wait(barrier, inner + outer + tp - 3)
+    pl.semaphore_wait(barrier, inner + outer - 1 + jnp.where(inside, 2 * CORES, CORES))
     send(GRAD, 0)
     loaded(1, own - 1)
     decays([(r, u) for u in range(1, own) for r in everyone])
@@ -233,6 +261,7 @@
 
     end = own - 1
     take(wgt_v, i_s.at[6])
+    w_near()
     take(k_v, i_s.at[7])
     for u in range(own):
         take(hid_v.at[rows(0, u, inner)], h_s.at[u])
@@ -241,13 +270,12 @@
         if u < end:
             send(STATE, u)
 
-    for r in range(1, tp):
-        w_copy(r).start()
     w_in[tpi] = wgt_v[pl.ds(pl.multiple_of(tpi * feat, feat), feat), :]
     mine = [(0, u) for u in range(own)]
     emit(GRAD, mine)
     emit(STATE, mine)
     w_acc[...] = jnp.zeros((dv, width), F32)
+    w_across()
 
     def offset(person):
         return lax.rem(y - person + inner, inner)
@@ -437,13 +465,13 @@
     loop(0, end, first_steps)
     combine_plane(GRAD, end)
     combine_all(GRAD, 0)
+    w_ends()
     finish_own(0)
     intra_all(end)
-    loop(1, end, second_steps)
+    loop(1, own, second_steps)
     send(STATE, end)
-    second_steps(end)
-    loop(0, end, third_steps)
-    combine_plane(STATE, end)
+    loop(0, end - 1, third_steps)
+    weigh(end - 1)
 
     finish_others(end)
     full = w_acc[...] + weight_terms(end)
@@ -451,6 +479,8 @@
         block = full[:, p * rows_sp:(p + 2) * rows_sp].T.astype(BF16)
         g_out[p] = block[:rows_sp]
         g_out[p + 1] = block[rows_sp:]
+    pass_states(end - 1)
+    combine_plane(STATE, end)
     for away_by in OFFSETS:
         g_copy(*away_by).start()
     loop(0, end - 1, fourth_steps)
@@ -458,7 +488,11 @@
     pass_states(end)
     forward(end)
     rest_others(end - 1)
-    take(w_in.at[pl.ds(0, tp - 1)], w_rs.at[0])
+
+    @pl.when(jnp.logical_not(inside))
+    def _():
+        take(w_in.at[pl.ds(0, CORES)], w_rs.at[2])
+
     loop(0, own, features)
     rest_others(end)
 
@@ -533,7 +567,7 @@
         dma((1,)), dma((2, own)),
         dma((1,)), dma((own,)),
         dma((1,)), dma((own,)),
-        dma((1,)), dma((1,)),
+        dma((1,)), dma((3,)),
         dma((1,)), dma((1,)),
     ]
     whole = pl.BlockSpec(memory_space=vmem)

time: 37.6 us -> 37 us (0.984)
  the two profiles are of different devices: /device:TPU:0 before, /device:TPU:1 now
where the time goes in v8:
time: 37 us; the launch traced here: 36.9 us
  Pallas kernels  36.2 us (98%)
  between operations  0.64 us (2%)
    pallas_call x1, Pallas kernels, shards(): pl.pallas_call(functools.partial(kernel, dims), out_shape=(vmem(flat, BF1...  34.9 us
    pallas_call x1, Pallas kernels, store(): pl.pallas_call(store_kernel, out_shape=tuple((jax.ShapeDtypeStruct(a.shap...  1.28 us

profile of v8, /device:TPU:1, one launch (start us, length us, event | category | flops | bytes accessed | tf_op | source)
XLA Modules:
  0.0 36.9 jit_solution(1440576763793334317)
XLA Ops:
  0.6 34.9 %shard_map.118 = (bf16[16,64,64]{2,1,0:T(8,128)(2,1)S(1)}, bf16[16,64,64]{2,1,0:T(8,128)(2,1)S(1)}, f32[16,64,64]{2,1,0:T(8,128)S(1)}, f32[16,64,64]{2,1,0:T(8,1...) custom-call(bf16[4,4,64,1024]{3,2,1,0:T(8,128)(2,1)} %bitcast.18, bf16[1024,128]{1,0:T(8,128)(2,1)} %wgt.1, ...), custom_call_target="tpu_custom_call" | custom-call | tf_op jit(solution)/shard_map/pallas_call | solution.py:578
  35.6 1.3 %shard_map.119 = (bf16[16,64,64]{2,1,0:T(8,128)(2,1)}, bf16[16,64,64]{2,1,0:T(8,128)(2,1)}, f32[16,64,64]{2,1,0:T(8,128)}, f32[16,64,64]{2,1,0:T(8,128)}, bf16[1...) custom-call(bf16[16,64,64]{2,1,0:T(8,128)(2,1)S(1)} %get-tuple-element.18.refs_0_, ...), custom_call_target="tpu_custom_call" | custom-call | tf_op jit(solution)/shard_map/pallas_call | solution.py:527

commit v9 on v8

--- a/solution.py
+++ b/solution.py
@@ -33,8 +33,8 @@
            val, cum, q_hats, k_ends, intra_q, intra_k, intra_v,
            a_out, a_in, e_out, e_in, local, b_out, b_in, c_out, c_in,
            d_all, w_in, w_acc, g_out, g_in,
-           i_s, h_s, a_ss, a_rs, e_ss, e_rs, b_ss, b_rs, c_ss, c_rs,
-           d_ss, d_rs, f_ss, f_rs, w_ss, w_rs, g_ss, g_rs):
+           i_s, h_s, x_ss, a_rs, e_ss, e_rs, b_ss, b_rs, c_rs,
+           d_rs, f_ss, f_rs, w_ss, w_rs, g_ss, g_rs):
     sp, tp, batch, length, dk, dv, width = dims
     inner, outer, own, xs = INNER, sp // INNER, batch // INNER, tp // CORES
     pack, feat, rows_sp, group = 2 * dk, width // tp, width // sp, INNER * length
@@ -134,7 +134,7 @@
                 w_copy((xs - 1 - x) * CORES + c, 2).start()
 
     def a_copy(kind, r, u):
-        return remote(a_out.at[kind, u, r - 1], a_in.at[kind, u, r], a_ss.at[0], a_rs.at[kind, u],
+        return remote(a_out.at[kind, u, r - 1], a_in.at[kind, u, r], x_ss.at[0], a_rs.at[kind, u],
                       sp=z * inner + owner(r))
 
     def e_copy(r):
@@ -149,13 +149,13 @@
                       b_ss.at[kind], b_rs.at[kind, u], sp=lax.rem(z + r, outer) * inner + y)
 
     def c_copy(kind, r, u):
-        return remote(c_out.at[kind, u, r], c_in.at[kind, u, r - 1], c_ss.at[0], c_rs.at[kind, u],
+        return remote(c_out.at[kind, u, r], c_in.at[kind, u, r - 1], x_ss.at[0], c_rs.at[kind, u],
                       sp=z * inner + lax.rem(y - r + inner, inner))
 
     def d_copies(r, u, count):
         at = rows(r, u, count)
         for k in FAR_FIRST:
-            remote(d_all.at[tpi, at], d_all.at[tpi, at], d_ss.at[0], d_rs.at[u],
+            remote(d_all.at[tpi, at], d_all.at[tpi, at], f_ss.at[0], d_rs.at[u],
                    tp=lax.rem(x + k, xs) * CORES + core).start()
         remote(d_all.at[tpi, at], d_all.at[tpi, at], f_ss.at[0], f_rs.at[u], tp=mate).start()
 
@@ -413,6 +413,39 @@
         for r in range(inner):
             o_h[batch_of(r, u)] = out[r * length:(r + 1) * length]
 
+    def prepare_rest(todo):
+        made = []
+        for r, u in todo:
+            b, at = batch_of(r, u), slot(r, u)
+            c = cum[at]
+            q, k = twice(q_v, r, u), twice(k_v, r, u)
+            dk_ = (jnp.exp(-c) * intra_k[at]
+                   + jnp.exp(ends(c) - c) * dot(val[rows(r, u)], arrived(GRAD, r, u)))
+            o_k[b] = (dk_[:, :dk] + dk_[:, dk:]).astype(BF16)
+            made.append(q * jnp.exp(c) * intra_q[at] - k * dk_)
+        for (r, u), known in zip(todo, made):
+            intra_k[slot(r, u)] = known
+
+    def close_rest(todo):
+        kept, terms = [], []
+        for r, u in todo:
+            at = slot(r, u)
+            state, grad = arrived(STATE, r, u), arrived(GRAD, r, u)
+            c = cum[at]
+            grow = jnp.exp(c)
+            cross = dot(cot_v[owner(r), u], state)
+            far = twice(q_v, r, u) * grow * cross
+            terms.append(intra_k[at] + far)
+            start = (jnp.sum(far, axis=0, keepdims=True)
+                     + jnp.exp(ends(c)) * jnp.sum(state.astype(F32) * grad.astype(F32), axis=0, keepdims=True))
+            kept.append((grow * (intra_q[at] + cross), start))
+        for (r, u), (dq, start), sums_ in zip(todo, kept, directed(strict, terms)):
+            b = batch_of(r, u)
+            decay_grad = start - sums_
+            o_q[b] = (dq[:, :dk] + dq[:, dk:]).astype(BF16)
+            o_f[b] = decay_grad[:, :dk]
+            o_b[b] = decay_grad[:, dk:]
+
     def finish_own(u):
         finish_values([(0, u)])
         d_copies(0, u, 1)
@@ -483,9 +516,11 @@
     combine_plane(STATE, end)
     for away_by in OFFSETS:
         g_copy(*away_by).start()
-    loop(0, end - 1, fourth_steps)
-    forward(end - 1)
-    pass_states(end)
+    loop(0, end - 1, rest_others)
+    combine_all(STATE, end)
+    prepare_rest([(r, end) for r in visitors])
+    loop(0, end, forward)
+    finish_rest([(0, end)])
     forward(end)
     rest_others(end - 1)
 
@@ -494,7 +529,8 @@
         take(w_in.at[pl.ds(0, CORES)], w_rs.at[2])
 
     loop(0, own, features)
-    rest_others(end)
+    take(c_in.at[STATE, end], c_rs.at[STATE, end])
+    close_rest([(r, end) for r in visitors])
 
     take(g_in, g_rs.at[0])
     acc = g_out[spi].astype(F32)
@@ -504,12 +540,10 @@
 
     take(w_in.at[pl.ds(0, tp - 1)], w_ss.at[0])
     take(e_in.at[pl.ds(1, inner - 1)], e_ss.at[0])
-    take(a_out, a_ss.at[0])
+    take(d_all.at[pl.ds(0, tp - 2)], x_ss.at[0])
     take(b_in.at[GRAD], b_ss.at[GRAD])
     take(b_in.at[STATE, :, :, pl.ds(0, fold)], b_ss.at[STATE])
-    take(c_in, c_ss.at[0])
-    take(d_all.at[pl.ds(0, xs - 1)], d_ss.at[0])
-    take(d_all.at[pl.ds(0, xs)], f_ss.at[0])
+    take(d_all.at[pl.ds(0, tp - 1)], f_ss.at[0])
     take(g_in, g_ss.at[0])
 
 
@@ -564,8 +598,8 @@
         dma((1,)), dma((2, own)),
         dma((1,)), dma((1,)),
         dma((2,)), dma((2, own)),
-        dma((1,)), dma((2, own)),
-        dma((1,)), dma((own,)),
+        dma((2, own)),
+        dma((own,)),
         dma((1,)), dma((own,)),
         dma((1,)), dma((3,)),
         dma((1,)), dma((1,)),

time: 37 us -> 37 us (level)
  no operation moved by 1% of the time
where the time goes in v9:
time: 37 us; the launch traced here: 36.9 us
  Pallas kernels  36.2 us (98%)
  between operations  0.64 us (2%)
    pallas_call x1, Pallas kernels, shards(): pl.pallas_call(functools.partial(kernel, dims), out_shape=(vmem(flat, BF1...  34.9 us
    pallas_call x1, Pallas kernels, store(): pl.pallas_call(store_kernel, out_shape=tuple((jax.ShapeDtypeStruct(a.shap...  1.28 us

profile of v9, /device:TPU:1, one launch (start us, length us, event | category | flops | bytes accessed | tf_op | source)
XLA Modules:
  0.0 36.9 jit_solution(14055532433166400963)
XLA Ops:
  0.6 34.9 %shard_map.118 = (bf16[16,64,64]{2,1,0:T(8,128)(2,1)S(1)}, bf16[16,64,64]{2,1,0:T(8,128)(2,1)S(1)}, f32[16,64,64]{2,1,0:T(8,128)S(1)}, f32[16,64,64]{2,1,0:T(8,1...) custom-call(bf16[4,4,64,1024]{3,2,1,0:T(8,128)(2,1)} %bitcast.18, bf16[1024,128]{1,0:T(8,128)(2,1)} %wgt.1, ...), custom_call_target="tpu_custom_call" | custom-call | tf_op jit(solution)/shard_map/pallas_call | solution.py:612
  35.6 1.3 %shard_map.119 = (bf16[16,64,64]{2,1,0:T(8,128)(2,1)}, bf16[16,64,64]{2,1,0:T(8,128)(2,1)}, f32[16,64,64]{2,1,0:T(8,128)}, f32[16,64,64]{2,1,0:T(8,128)}, bf16[1...) custom-call(bf16[16,64,64]{2,1,0:T(8,128)(2,1)S(1)} %get-tuple-element.18.refs_0_, ...), custom_call_target="tpu_custom_call" | custom-call | tf_op jit(solution)/shard_map/pallas_call | solution.py:561

commit v10 on v9

--- a/solution.py
+++ b/solution.py
@@ -15,7 +15,7 @@
 GRAD, STATE = 0, 1
 FAR_FIRST = (2, 1, 3)
 OFFSETS = sorted(((dz, dy) for dz in range(4) for dy in range(4) if dz or dy),
-                 key=lambda d: -sum(min(v, 4 - v) for v in d))
+                 key=lambda d: (-min(d[1], 4 - d[1]), -min(d[0], 4 - d[0])))
 
 
 def dot(a, b, ca=1, cb=0):

time: 37 us -> 37 us (level)
  no operation moved by 1% of the time
where the time goes in v10:
time: 37 us; the launch traced here: 36.9 us
  Pallas kernels  36.3 us (98%)
  between operations  0.64 us (2%)
    pallas_call x1, Pallas kernels, shards(): pl.pallas_call(functools.partial(kernel, dims), out_shape=(vmem(flat, BF1...  35 us
    pallas_call x1, Pallas kernels, store(): pl.pallas_call(store_kernel, out_shape=tuple((jax.ShapeDtypeStruct(a.shap...  1.28 us

profile of v10, /device:TPU:1, one launch (start us, length us, event | category | flops | bytes accessed | tf_op | source)
XLA Modules:
  0.0 36.9 jit_solution(7603798051131271426)
XLA Ops:
  0.6 35.0 %shard_map.118 = (bf16[16,64,64]{2,1,0:T(8,128)(2,1)S(1)}, bf16[16,64,64]{2,1,0:T(8,128)(2,1)S(1)}, f32[16,64,64]{2,1,0:T(8,128)S(1)}, f32[16,64,64]{2,1,0:T(8,1...) custom-call(bf16[4,4,64,1024]{3,2,1,0:T(8,128)(2,1)} %bitcast.18, bf16[1024,128]{1,0:T(8,128)(2,1)} %wgt.1, ...), custom_call_target="tpu_custom_call" | custom-call | tf_op jit(solution)/shard_map/pallas_call | solution.py:612
  35.6 1.3 %shard_map.119 = (bf16[16,64,64]{2,1,0:T(8,128)(2,1)}, bf16[16,64,64]{2,1,0:T(8,128)(2,1)}, f32[16,64,64]{2,1,0:T(8,128)}, f32[16,64,64]{2,1,0:T(8,128)}, bf16[1...) custom-call(bf16[16,64,64]{2,1,0:T(8,128)(2,1)S(1)} %get-tuple-element.18.refs_0_, ...), custom_call_target="tpu_custom_call" | custom-call | tf_op jit(solution)/shard_map/pallas_call | solution.py:561

commit v11 on v9

--- a/solution.py
+++ b/solution.py
@@ -475,8 +475,8 @@
 
     def second_steps(u):
         combine_all(GRAD, u)
+        combine_plane(STATE, u - 1)
         finish_own(u)
-        combine_plane(STATE, u - 1)
 
     def weigh(u):
         finish_others(u)

time: 37 us -> 37 us (level)
  no operation moved by 1% of the time
where the time goes in v11:
time: 37 us; the launch traced here: 36.9 us
  Pallas kernels  36.2 us (98%)
  between operations  0.64 us (2%)
    pallas_call x1, Pallas kernels, shards(): pl.pallas_call(functools.partial(kernel, dims), out_shape=(vmem(flat, BF1...  34.9 us
    pallas_call x1, Pallas kernels, store(): pl.pallas_call(store_kernel, out_shape=tuple((jax.ShapeDtypeStruct(a.shap...  1.28 us

profile of v11, /device:TPU:1, one launch (start us, length us, event | category | flops | bytes accessed | tf_op | source)
XLA Modules:
  0.0 36.9 jit_solution(15665474178379247984)
XLA Ops:
  0.6 34.9 %shard_map.118 = (bf16[16,64,64]{2,1,0:T(8,128)(2,1)S(1)}, bf16[16,64,64]{2,1,0:T(8,128)(2,1)S(1)}, f32[16,64,64]{2,1,0:T(8,128)S(1)}, f32[16,64,64]{2,1,0:T(8,1...) custom-call(bf16[4,4,64,1024]{3,2,1,0:T(8,128)(2,1)} %bitcast.18, bf16[1024,128]{1,0:T(8,128)(2,1)} %wgt.1, ...), custom_call_target="tpu_custom_call" | custom-call | tf_op jit(solution)/shard_map/pallas_call | solution.py:612
  35.6 1.3 %shard_map.119 = (bf16[16,64,64]{2,1,0:T(8,128)(2,1)}, bf16[16,64,64]{2,1,0:T(8,128)(2,1)}, f32[16,64,64]{2,1,0:T(8,128)}, f32[16,64,64]{2,1,0:T(8,128)}, bf16[1...) custom-call(bf16[16,64,64]{2,1,0:T(8,128)(2,1)S(1)} %get-tuple-element.18.refs_0_, ...), custom_call_target="tpu_custom_call" | custom-call | tf_op jit(solution)/shard_map/pallas_call | solution.py:561
